TPU v7x, 256 devices: a whole 4x4x8 slice. The times are simulated.
256 devices in a mesh: kv: 32 (over z, x), tp: 8 (over y, core).
Axes of the slice: x: 4, y: 4, z: 8, core: 2. Of those that a mesh axis runs over, the one named last changes fastest.
Arguments:
- queries: bfloat16 [4096, 2048], P('kv', 'tp'), may hold values from -6 to 6
- keys: bfloat16 [4096, 2048], P('kv', 'tp'), may hold values from -6 to 6
- values: bfloat16 [4096, 2048], P('kv', 'tp'), may hold values from -6 to 6
- attended: bfloat16 [4096, 2048], P('kv', 'tp'), may hold values from -6 to 6
- cotangent: bfloat16 [4096, 2048], P('kv', 'tp'), may hold values from -96 to 96
- log_totals: float32 [32, 4096], P('tp', 'kv'), may hold values from 4 to 7
- block_picks: int32 [32, 64, 8], P('tp', 'kv'), may hold values from -1 to 62, as said below
- normed: bfloat16 [4096, 4096], P('kv', 'tp'), may hold values from -6 to 6
Outputs:
- grad_queries: bfloat16 [4096, 2048], P('kv', 'tp')
- grad_keys: bfloat16 [4096, 2048], P('kv', 'tp')
- grad_values: bfloat16 [4096, 2048], P('kv', 'tp')
- grad_weight: float32 [4096, 2048], P('kv', 'tp')
Inputs may be any that keep to these rules, and one draw needn't show every extreme that they name: `block_picks`: row c of head h names at most 8 distinct blocks below c, followed by -1 in the other slots. One key block is named by at most 16 query blocks of one head, and in every draw each head has a block named exactly 16 times.
All inputs are finite; a program needn't handle non-finite values.
Results may differ from a plain program's by a relative error of at most 0.0069.
Values may be sent and summed in bfloat16 or wider, within the bound.
A program may use at most 128 MiB of HBM per device.

v0:
```python
import jax
import jax.numpy as jnp
from jax import lax
from jax.sharding import PartitionSpec as P

BLOCK = 64


def in_one_piece(arrays, axis, dim, along):
    widths = [a.shape[along] for a in arrays]
    both = jnp.concatenate(arrays, axis=along)
    filled = lax.all_gather(both, axis, axis=dim, tiled=True)
    return tuple(jnp.split(filled, [sum(widths[:k]) for k in range(1, len(widths))], axis=along))


def from_everyone(shard, axis):
    copies = jnp.broadcast_to(shard, (lax.axis_size(axis), *shard.shape))
    return lax.all_to_all(copies, axis, split_axis=0, concat_axis=0, tiled=True)


def laid_out(parts, dim):
    parts = jnp.moveaxis(parts, 0, dim)
    dims = parts.shape
    return parts.reshape(*dims[:dim], dims[dim] * dims[dim + 1], *dims[dim + 2 :])


def gathered_copies(shard, axis, dim):
    parts = from_everyone(shard, axis)
    return laid_out(parts, dim)


def cut_along(shard, dim, size):
    dims = shard.shape
    parts = shard.reshape(*dims[:dim], size, dims[dim] // size, *dims[dim + 1 :])
    return jnp.moveaxis(parts, dim, 0)


def summed_on_arrival(shard, axis, dim):
    parts = cut_along(shard, dim, lax.axis_size(axis))
    arrived = lax.all_to_all(parts, axis, split_axis=0, concat_axis=0, tiled=True)
    return arrived.astype(jnp.float32).sum(axis=0)


def tile_terms(q_tile, k_tile, v_tile, g_tile, log_total, row_dots, allowed):
    scale = q_tile.shape[-1] ** (-0.5)
    scores = (
        jnp.einsum("...qd,...kd->...qk", q_tile, k_tile, preferred_element_type=jnp.float32) * scale
    )
    probs = jnp.where(allowed, jnp.exp(scores - log_total[..., None]), 0.0)
    probs_low = probs.astype(jnp.bfloat16)
    grad_v = jnp.einsum("...qk,...qd->...kd", probs_low, g_tile, preferred_element_type=jnp.float32)
    grad_p = jnp.einsum("...qd,...kd->...qk", g_tile, v_tile, preferred_element_type=jnp.float32)
    grad_s = (probs * (grad_p - row_dots[..., None])).astype(jnp.bfloat16)
    grad_q = (
        jnp.einsum("...qk,...kd->...qd", grad_s, k_tile, preferred_element_type=jnp.float32) * scale
    )
    grad_k = (
        jnp.einsum("...qk,...qd->...kd", grad_s, q_tile, preferred_element_type=jnp.float32) * scale
    )
    return (grad_q, grad_k, grad_v)


def add_by_block(tiles, segments, block_total):
    onehot = (segments[..., None] == jnp.arange(block_total)).astype(jnp.float32)
    return jnp.einsum("hnb,hnkd->hbkd", onehot, tiles, precision=lax.Precision.HIGHEST)


def local(queries, keys, values, attended, cotangent, log_totals, block_picks, normed):
    tok_rows, row_width = queries.shape
    head_count = log_totals.shape[0]
    head_size = row_width // head_count
    local_blocks = tok_rows // BLOCK
    kv_count = lax.axis_size("kv")
    all_blocks = local_blocks * kv_count

    def by_head(matrix, blocks):
        return matrix.reshape(blocks, BLOCK, head_count, head_size).transpose(2, 0, 1, 3)

    def to_rows(tensor):
        return tensor.transpose(1, 2, 0, 3).reshape(tensor.shape[1] * BLOCK, row_width)

    q_heads = by_head(queries, local_blocks)
    k_heads = by_head(keys, local_blocks)
    v_heads = by_head(values, local_blocks)
    g_heads = by_head(cotangent, local_blocks)
    o_heads = by_head(attended, local_blocks)
    log_heads = log_totals.reshape(head_count, local_blocks, BLOCK)
    row_dots = jnp.einsum("hbqd,hbqd->hbq", g_heads, o_heads, preferred_element_type=jnp.float32)
    causal = jnp.tril(jnp.ones((BLOCK, BLOCK), bool))
    dq_diag, dk_diag, dv_diag = tile_terms(
        q_heads, k_heads, v_heads, g_heads, log_heads, row_dots, causal
    )
    q_all, g_all = in_one_piece((queries, cotangent), "kv", 0, 1)
    log_all, dots_all = in_one_piece(
        (log_totals, row_dots.reshape(head_count, tok_rows)), "kv", 1, 0
    )
    picks_all = gathered_copies(block_picks, "kv", 1)
    most = max(2, all_blocks // 4)
    own_ids = lax.axis_index("kv") * local_blocks + jnp.arange(local_blocks)
    matched = jnp.any(picks_all[:, :, :, None] == own_ids, axis=2)
    position = jnp.cumsum(matched.astype(jnp.int32), axis=1) - 1
    slot_hit = matched[..., None] & (position[..., None] == jnp.arange(most))
    listed = jnp.sum(jnp.where(slot_hit, jnp.arange(all_blocks)[None, :, None, None], 0), axis=1)
    filled = jnp.any(slot_hit, axis=1)
    q_blocks = by_head(q_all, all_blocks)
    g_blocks = by_head(g_all, all_blocks)
    log_blocks = log_all.reshape(head_count, all_blocks, BLOCK)
    dots_blocks = dots_all.reshape(head_count, all_blocks, BLOCK)
    q_sel = jax.vmap(lambda t, i: t[i])(q_blocks, listed)
    g_sel = jax.vmap(lambda t, i: t[i])(g_blocks, listed)
    l_sel = jax.vmap(lambda t, i: t[i])(log_blocks, listed)
    d_sel = jax.vmap(lambda t, i: t[i])(dots_blocks, listed)
    tile_shape = q_sel.shape
    k_rep = jnp.broadcast_to(k_heads[:, :, None], tile_shape)
    v_rep = jnp.broadcast_to(v_heads[:, :, None], tile_shape)
    allowed = jnp.broadcast_to(filled[..., None, None], tile_shape[:4] + (BLOCK,))
    dq_sel, dk_sel, dv_sel = tile_terms(q_sel, k_rep, v_rep, g_sel, l_sel, d_sel, allowed)
    grad_k = to_rows(dk_diag + jnp.sum(dk_sel, axis=2))
    grad_v = to_rows(dv_diag + jnp.sum(dv_sel, axis=2))
    segments = jnp.where(filled, listed, all_blocks).reshape(head_count, local_blocks * most)
    dq_blocks = add_by_block(
        dq_sel.reshape(head_count, local_blocks * most, BLOCK, head_size), segments, all_blocks
    )
    dq_full = to_rows(dq_blocks)
    remote_q = summed_on_arrival(dq_full.astype(jnp.bfloat16), "kv", 0)
    grad_queries = (remote_q + to_rows(dq_diag)).astype(jnp.bfloat16)
    full_hidden = lax.all_gather(normed, "tp", axis=1, tiled=True)
    grad_weight = summed_on_arrival(
        lax.dot_general(
            full_hidden, grad_queries, (((0,), (0,)), ((), ())), preferred_element_type=jnp.float32
        ).astype(jnp.bfloat16),
        "kv",
        0,
    )
    return (grad_queries, grad_k.astype(jnp.bfloat16), grad_v.astype(jnp.bfloat16), grad_weight)


def solution(mesh):
    in_specs = (
        P("kv", "tp"),
        P("kv", "tp"),
        P("kv", "tp"),
        P("kv", "tp"),
        P("kv", "tp"),
        P("tp", "kv"),
        P("tp", "kv", None),
        P("kv", "tp"),
    )
    out_specs = (P("kv", "tp"), P("kv", "tp"), P("kv", "tp"), P("kv", "tp"))
    return jax.shard_map(local, mesh=mesh, in_specs=in_specs, out_specs=out_specs, check_vma=False)
```

profile of v0, /device:TPU:2, one launch (start us, length us, event | category | flops | bytes accessed | tf_op | source)
XLA Modules:
  0.0 283.7 jit_solution(4244892745333375316)
XLA Ops:
  11.0 11.6 %all-to-all-start = ((s32[32,4,2,8]{3,2,1,0:T(2,128)}), s32[32,4,2,8]{3,2,1,0:T(2,128)S(1)}, u32[]{:S(2)}, u32[]{:S(2)}) async-start(s32[32,4,2,8]{3,2,1,0:T(2,128)} %broadcast_in_dim.38), calls=%async_computation | async-start | bytes 262144 | tf_op jit(solution)/shard_map/all_to_all | solution.py:18
  25.7 42.8 %all_gather.10 = f32[8,4096]{1,0:T(8,128)S(1)} all-gather(f32[8,128]{1,0:T(8,128)S(1)} %pad_maximum_fusion.1), channel_id=1, replica_groups=mesh['kv'=32,'tp'=8] {'kv'}, dimensions={1}, use_global_device_ids=true | all-gather | bytes 135168 | tf_op jit(solution)/shard_map/all_gather | solution.py:12
  74.5 21.0 %all-gather.3.cloned.1.call-done = bf16[4096,512]{1,0:T(8,128)(2,1)} async-done(((bf16[128,512]{1,0:T(8,128)(2,1)}), bf16[4096,512]{1,0:T(8,128)(2,1)}) %all-gather.3.cloned.1.call-update) | async-done | bytes 4194320 | tf_op jit(solution)/shard_map/all_gather | solution.py:12
  95.5 3.8 %fusion.49 = (bf16[4096,256]{1,0:T(8,128)(2,1)}, bf16[4096,256]{1,0:T(8,128)(2,1)S(1)}) fusion(bf16[4096,512]{1,0:T(8,128)(2,1)} %all-gather.3.cloned.1.call-done), kind=kLoop, calls=%fused_computation.80 | loop fusion | bytes 8388608 | tf_op jit(solution)/shard_map/split | solution.py:13
  99.3 7.1 %reshape.144 = bf16[64,64,4,64]{3,2,1,0:T(4,128)(2,1)} reshape(bf16[4096,256]{1,0:T(8,128)(2,1)} %get-tuple-element.16) | data formatting | bytes 4194304 | tf_op jit(solution)/shard_map/reshape | solution.py:77
  106.4 5.3 %copy.186 = bf16[64,64,4,64]{3,1,0,2:T(8,128)(2,1)} copy(bf16[64,64,4,64]{3,2,1,0:T(4,128)(2,1)} %reshape.144) | data formatting | bytes 4194304 | tf_op jit(solution)/shard_map/reshape | solution.py:77
  111.7 4.5 %gather_fusion.2 = bf16[128,64,64]{2,1,0:T(8,128)(2,1)} fusion(bf16[4,64,64,64]{3,2,1,0:T(8,128)(2,1)} %bitcast.79, s32[128]{0:T(128)S(1)} %reshape.114), kind=kCustom, calls=%fused_computation.2 | custom fusion | bytes 2098176 | tf_op jit(solution)/shard_map/vmap()/gather | solution.py:110
  116.2 3.3 %reshape.143 = bf16[64,64,4,64]{3,2,1,0:T(4,128)(2,1)} reshape(bf16[4096,256]{1,0:T(8,128)(2,1)S(1)} %get-tuple-element.17) | data formatting | bytes 4194304 | tf_op jit(solution)/shard_map/reshape | solution.py:77
  119.4 5.3 %copy.187 = bf16[64,64,4,64]{3,1,0,2:T(8,128)(2,1)} copy(bf16[64,64,4,64]{3,2,1,0:T(4,128)(2,1)} %reshape.143) | data formatting | bytes 4194304 | tf_op jit(solution)/shard_map/reshape | solution.py:77
  124.7 3.3 %gather_fusion = bf16[128,64,64]{2,1,0:T(8,128)(2,1)S(1)} fusion(bf16[4,64,64,64]{3,2,1,0:T(8,128)(2,1)} %bitcast.78, s32[128]{0:T(128)S(1)} %reshape.114), kind=kCustom, calls=%fused_computation | custom fusion | bytes 2098176 | tf_op jit(solution)/shard_map/vmap()/gather | solution.py:109
  129.2 1.9 copy-done.1
  131.1 3.1 %multiply_convert_fusion = bf16[4,2,16,64,64]{4,3,2,1,0:T(8,128)(2,1)S(1)} fusion(f32[4,2,16,64,64]{4,3,2,1,0:T(8,128)S(1)} %fusion.28, bf16[4,2,16,64,64]{4,3,2,1,0:T(8,128)(2,1)S(1)} %bitcast.84, f32[4,2,16,64]{3,2,1,0:T(8,128)S(1)} %bitcast.92, f32[4,2,16,64]{3,2,1,0:T(8,128)S(1)} %bitcast.90, pred[4,2,16]{2,1,0:T(4,128)(4,1)S(1)} %fusion.40, ...), kind=kOutput, calls=%fused_computation.13 | convolution fusion | flops 70254592 | bytes 4325504 | tf_op jit(solution)/shard_map/...qd,...kd->...qk/dot_general | solution.py:52
  135.6 7.0 %convert_bitcast_fusion = bf16[64,64,4,64]{3,0,1,2:T(8,128)(2,1)} fusion(f32[4,32,64,64]{3,2,1,0:T(8,128)S(1)} %bitcast.77, s32[4,32]{1,0:T(4,128)S(1)} %select_n.40), kind=kOutput, calls=%fused_computation.12 | convolution fusion | flops 403709952 | bytes 4194816 | tf_op jit(solution)/shard_map/hnb,hnkd->hbkd/dot_general | solution.py:65
  142.6 7.4 %copy.119 = bf16[64,64,4,64]{1,0,3,2:T(8,128)(2,1)} copy(bf16[64,64,4,64]{3,0,1,2:T(8,128)(2,1)} %convert_bitcast_fusion) | data formatting | bytes 4194304 | tf_op jit(solution)/shard_map/convert_element_type | solution.py:125
  150.0 6.3 %convert_element_type.67 = bf16[32,128,256]{1,0,2:T(8,128)(2,1)} reshape(bf16[64,64,4,64]{1,0,3,2:T(8,128)(2,1)} %copy.119) | data formatting | bytes 4194304 | tf_op jit(solution)/shard_map/convert_element_type | solution.py:125
  156.2 3.8 %copy.120 = bf16[32,128,256]{1,2,0:T(8,128)(2,1)} copy(bf16[32,128,256]{1,0,2:T(8,128)(2,1)} %convert_element_type.67) | data formatting | bytes 4194304 | tf_op jit(solution)/shard_map/convert_element_type | solution.py:125
  160.0 6.9 %all-to-all-start.1 = ((bf16[32,128,256]{1,2,0:T(8,128)(2,1)}), bf16[32,128,256]{1,2,0:T(8,128)(2,1)}, u32[]{:S(2)}, u32[]{:S(2)}) async-start(bf16[32,128,256]{1,2,0:T(8,128)(2,1)} %copy.120), calls=%async_computation.1 | async-start | bytes 4194304 | tf_op jit(solution)/shard_map/all_to_all | solution.py:40
  168.7 45.5 %all-to-all-done.1 = bf16[32,128,256]{1,2,0:T(8,128)(2,1)} async-done(((bf16[32,128,256]{1,2,0:T(8,128)(2,1)}), bf16[32,128,256]{1,2,0:T(8,128)(2,1)}, u32[]{:S(2)}, u32[]{:S(2)}) %all-to-all-start.1) | async-done | bytes 2097184 | tf_op jit(solution)/shard_map/all_to_all | solution.py:40
  216.2 1.9 fusion.11
  218.1 1.9 copy.188
  220.1 6.3 %all-to-all-start.2 = ((bf16[32,128,256]{1,2,0:T(8,128)(2,1)}), bf16[32,128,256]{1,2,0:T(8,128)(2,1)}, u32[]{:S(2)}, u32[]{:S(2)}) async-start(bf16[32,128,256]{1,2,0:T(8,128)(2,1)} %bitcast.82), calls=%async_computation.2 | async-start | bytes 4194304 | tf_op jit(solution)/shard_map/all_to_all | solution.py:40
  226.4 2.6 multiply_reduce_fusion
  230.1 4.6 %fusion.18 = f32[4,2,64,64]{3,2,1,0:T(8,128)S(1)} fusion(bf16[4,2,16,64,64]{4,3,2,1,0:T(8,128)(2,1)} %bitcast.83, f32[4,2,16,64,64]{4,3,2,1,0:T(8,128)} %copy-done.1, f32[4,2,16,64]{3,2,1,0:T(8,128)S(1)} %bitcast.91, pred[4,2,16]{2,1,0:T(4,128)(4,1)S(1)} %fusion.40), kind=kOutput, calls=%fused_computation.35 | convolution fusion | flops 69206016 | bytes 3309696 | tf_op jit(solution)/shard_map/...qk,...qd->...kd/dot_general | solution.py:51
  236.5 37.0 %all-to-all-done.2 = bf16[32,128,256]{1,2,0:T(8,128)(2,1)} async-done(((bf16[32,128,256]{1,2,0:T(8,128)(2,1)}), bf16[32,128,256]{1,2,0:T(8,128)(2,1)}, u32[]{:S(2)}, u32[]{:S(2)}) %all-to-all-start.2) | async-done | bytes 2097184 | tf_op jit(solution)/shard_map/all_to_all | solution.py:40
  (69 shorter events, 23.8 us)
Async XLA Ops:
  8.0 87.5 %all-gather.3.cloned.1.call-start = ((), (), s32[]{:S(2)}) async-start(), calls=%async_computation.3 | async-start | bytes 4325376 | tf_op jit(solution)/shard_map/all_gather | solution.py:12
  11.0 59.8 %all-to-all-start = ((s32[32,4,2,8]{3,2,1,0:T(2,128)}), s32[32,4,2,8]{3,2,1,0:T(2,128)S(1)}, u32[]{:S(2)}, u32[]{:S(2)}) async-start(s32[32,4,2,8]{3,2,1,0:T(2,128)} %broadcast_in_dim.38), calls=%async_computation | async-start | bytes 262144 | tf_op jit(solution)/shard_map/all_to_all | solution.py:18
  128.0 3.2 %copy-start.2 = (bf16[128,64,64]{2,1,0:T(8,128)(2,1)S(1)}, bf16[128,64,64]{2,1,0:T(8,128)(2,1)}, u32[]{:S(2)}) copy-start(bf16[128,64,64]{2,1,0:T(8,128)(2,1)} %gather_fusion.2) | copy-start | bytes 3145732
  129.2 1.9 copy-start.1
  134.2 1.3 copy-start
  156.2 11.3 %copy-start.4 = (f32[4,128]{1,0:T(4,128)S(1)}, f32[4,128]{1,0:T(4,128)}, u32[]{:S(2)}) copy-start(f32[4,128]{1,0:T(4,128)} %param.13) | copy-start | bytes 6148
  156.2 11.4 %copy-start.3 = (bf16[128,256]{1,0:T(8,128)(2,1)S(1)}, bf16[128,256]{1,0:T(8,128)(2,1)}, u32[]{:S(2)}) copy-start(bf16[128,256]{1,0:T(8,128)(2,1)} %param.8) | copy-start | bytes 196612
  160.0 54.2 %all-to-all-start.1 = ((bf16[32,128,256]{1,2,0:T(8,128)(2,1)}), bf16[32,128,256]{1,2,0:T(8,128)(2,1)}, u32[]{:S(2)}, u32[]{:S(2)}) async-start(bf16[32,128,256]{1,2,0:T(8,128)(2,1)} %copy.120), calls=%async_computation.1 | async-start | bytes 4194304 | tf_op jit(solution)/shard_map/all_to_all | solution.py:40
  167.0 49.2 %all-gather.5.cloned.1.call-start = ((), (), s32[]{:S(2)}) async-start(), calls=%async_computation.4 | async-start | bytes 1179648 | tf_op jit(solution)/shard_map/all_gather | solution.py:127
  220.1 53.5 %all-to-all-start.2 = ((bf16[32,128,256]{1,2,0:T(8,128)(2,1)}), bf16[32,128,256]{1,2,0:T(8,128)(2,1)}, u32[]{:S(2)}, u32[]{:S(2)}) async-start(bf16[32,128,256]{1,2,0:T(8,128)(2,1)} %bitcast.82), calls=%async_computation.2 | async-start | bytes 4194304 | tf_op jit(solution)/shard_map/all_to_all | solution.py:40
Sparse Core Ops, SparseCore 0:
  12.0 83.4 all-gather.2
Sparse Core Ops, SparseCore 1:
  169.3 26.6 all-gather.4
where the time goes:
time: 285 us; the launch traced here: 284 us
  waiting for transfers between devices  104 us (36%)
  local copies, waits for them, and re-layouts  66.9 us (23%)
  blocking collectives  42.8 us (15%)
  starting transfers between devices  25.2 us (9%)
  matrix products  22.1 us (8%)
  between operations  15.8 us (6%)
  other arithmetic  7.1 us (2%)
    all_to_all x2, waiting for transfers between devices, summed_on_arrival(): lax.all_to_all(parts, axis, split_axis=0, concat_axis=0, tiled=True)  82.6 us
    all_gather x1, blocking collectives, in_one_piece(): filled = lax.all_gather(both, axis, axis=dim, tiled=True)  42.8 us
    reshape x11, local copies, waits for them, and re-layouts, by_head(): matrix.reshape(blocks, BLOCK, head_count, head_size).transpose(2, 0, 1, 3)  24.9 us
    all_gather x1, waiting for transfers between devices, in_one_piece(): filled = lax.all_gather(both, axis, axis=dim, tiled=True)  21 us
    convert_element_type x3, local copies, waits for them, and re-layouts, local(): remote_q = summed_on_arrival(dq_full.astype(jnp.bfloat16), 'kv', 0)  17.4 us
    all_to_all x2, starting transfers between devices, summed_on_arrival(): lax.all_to_all(parts, axis, split_axis=0, concat_axis=0, tiled=True)  13.3 us
    all_to_all x1, starting transfers between devices, from_everyone(): return lax.all_to_all(copies, axis, split_axis=0, concat_axis=0, tiled=True)  11.6 us
    dot_general x1, matrix products, add_by_block(): jnp.einsum('hnb,hnkd->hbkd', onehot, tiles, precision=lax.Precision.HIGHEST)  6.99 us
  transfers between devices with their start and end apart: 5, of which 3 were waited for; matrix products, arithmetic and copies ran while one was open for 8% of the time, Pallas kernels for 0%

commit v1 on v0

v1 whole, which is shorter than its diff:
```python
import functools
import math

import jax
import jax.numpy as jnp
from jax import lax
from jax.experimental import pallas as pl
from jax.experimental.pallas import tpu as pltpu
from jax.sharding import PartitionSpec as P

MESH = pl.DeviceIdType.MESH
BLOCK = 64
NZ, NX, NT = 8, 4, 8
ROWS = 128
WIDTH = 256
HEADS, DH = 4, 64
SEL = 8
FEATS = 128
KB = 2 * NX
NEVER = 1e30
F32, BF16 = jnp.float32, jnp.bfloat16

UP, DOWN = NZ // 2, NZ // 2 - 1


def up_slot(s):
    return 2 * s - 1


def down_slot(s):
    return 2 * s if s < NZ // 2 else NZ - 1


OFFSETS = [0] + [None] * (NZ - 1)
for _s in range(1, NZ // 2 + 1):
    OFFSETS[up_slot(_s)] = -_s
for _s in range(1, NZ // 2):
    OFFSETS[down_slot(_s)] = _s
PAIR = [0] + [OFFSETS.index(-o) if -o in OFFSETS else NZ - 1 for o in OFFSETS[1:]]


def nt_dot(a, b):
    return lax.dot_general(a, b, (((1,), (1,)), ((), ())), preferred_element_type=F32)


def nn_dot(a, b):
    return lax.dot_general(a, b, (((1,), (0,)), ((), ())), preferred_element_type=F32)


def diagonal_heads(m):
    lane_head = lax.broadcasted_iota(jnp.int32, (DH, WIDTH), 1) // DH
    out = m[(HEADS - 1) * DH :]
    for h in range(HEADS - 1):
        out = jnp.where(lane_head == h, m[h * DH : (h + 1) * DH], out)
    return out


def kernel(
    q_ref, k_ref, v_ref, o_ref, g_ref, l_ref, pick_ref, n_ref,
    gq_ref, gk_ref, gv_ref, gw_ref,
    qa, ga, lm, pk, kx, vx, kbd, vbd, kbt, ps, ds, dqs, dqr, dq0,
    nx, nt, ntt, dqx, dks, dvs, dkr, dvr, dk0, dv0, gws, gwr, gw0,
    send_sem, recv_sem,
):
    kv = lax.axis_index("kv")
    t = lax.axis_index("tp")
    a = kv // NX
    b = kv % NX
    scale = DH**-0.5
    log2e = 1.0 / math.log(2.0)

    def at_z(off):
        return {"kv": ((a + NZ + off) % NZ) * NX + b, "tp": t}

    def at_x(r):
        return {"kv": a * NX + (b + r) % NX, "tp": t}

    def at_t(r):
        return {"kv": kv, "tp": (t + r) % NT}

    started = []
    counts = [0]

    def sems(n):
        first = counts[0]
        counts[0] += n
        return first

    S_Q, S_L, S_P, S_G = sems(NZ), sems(NZ), sems(NZ), sems(NZ)
    S_K, S_V, S_N, S_T = sems(NX), sems(NX), sems(NX), sems(NT)
    S_DQ, S_DK, S_DV, S_X, S_W = sems(NZ), sems(NX), sems(NX), sems(NX), sems(NZ)

    def send(src, dst, at_mine, at_theirs, dev):
        copy = pltpu.make_async_remote_copy(
            src_ref=src, dst_ref=dst, send_sem=send_sem.at[at_mine], recv_sem=recv_sem.at[at_theirs],
            device_id=dev, device_id_type=MESH,
        )
        copy.start()
        started.append(copy)

    def arrived(dst, at_mine, dev):
        pltpu.make_async_remote_copy(
            src_ref=dst, dst_ref=dst, send_sem=send_sem.at[at_mine], recv_sem=recv_sem.at[at_mine],
            device_id=dev, device_id_type=MESH,
        ).wait_recv()

    def slot_rows(slot):
        return pl.ds(slot * ROWS, ROWS)

    barrier = pltpu.get_barrier_semaphore()
    for off in range(1, NZ):
        pl.semaphore_signal(barrier, inc=1, device_id=at_z(off), device_id_type=MESH)
    for r in range(1, NX):
        pl.semaphore_signal(barrier, inc=1, device_id=at_x(r), device_id_type=MESH)
    for r in range(1, NT):
        pl.semaphore_signal(barrier, inc=1, device_id=at_t(r), device_id_type=MESH)

    lane = lax.broadcasted_iota(jnp.int32, (8, ROWS), 1)
    sub = lax.broadcasted_iota(jnp.int32, (8, ROWS), 0)
    for h in range(HEADS):
        rows = jnp.zeros((8, ROWS), jnp.int32)
        for s in range(SEL):
            spread = jnp.where(lane < BLOCK, pick_ref[h, 0, s], pick_ref[h, 1, s])
            rows = jnp.where(sub == s, spread, rows)
        pk[0, h * 8 : (h + 1) * 8, :] = rows
    prod = g_ref[...].astype(F32) * o_ref[...].astype(F32)
    high = prod.astype(BF16)
    low = (prod - high.astype(F32)).astype(BF16)
    ones = (
        lax.broadcasted_iota(jnp.int32, (8, WIDTH), 1) // DH == lax.broadcasted_iota(jnp.int32, (8, WIDTH), 0)
    ).astype(BF16)
    dots = nt_dot(ones, high) + nt_dot(ones, low)
    lm[0, 0:HEADS, :] = l_ref[...] * log2e
    lm[0, HEADS : 2 * HEADS, :] = dots[0:HEADS]
    qa[slot_rows(0), :] = q_ref[...]
    ga[slot_rows(0), :] = g_ref[...]

    pl.semaphore_wait(barrier, (NZ - 1) + (NX - 1) + (NT - 1))

    def ring(s, down, first, ref, own, by_rows):
        slot_of = down_slot if down else up_slot
        there = slot_of(s + 1)
        dst = ref.at[slot_rows(there), :] if by_rows else ref.at[there]
        if s == 0:
            src = own
        else:
            src = ref.at[slot_rows(slot_of(s)), :] if by_rows else ref.at[slot_of(s)]
        send(src, dst, first + there, first + there, at_z(-1 if down else 1))

    def ring_arrived(s, down, first, ref, by_rows):
        slot = (down_slot if down else up_slot)(s)
        dst = ref.at[slot_rows(slot), :] if by_rows else ref.at[slot]
        arrived(dst, first + slot, at_z(1 if down else -1))

    streams = (
        (S_Q, qa, q_ref, True, UP, DOWN),
        (S_L, lm, lm.at[0], False, UP, DOWN),
        (S_P, pk, pk.at[0], False, UP, DOWN),
        (S_G, ga, g_ref, True, DOWN, UP),
    )

    def ring_step(s):
        for first, ref, own, by_rows, up, down in streams:
            for going_down, limit in ((False, up), (True, down)):
                if 0 < s <= limit:
                    ring_arrived(s, going_down, first, ref, by_rows)
                if s < limit:
                    ring(s, going_down, first, ref, own, by_rows)

    ring_step(0)
    for r in (1, 3, 2):
        send(k_ref, kx.at[NX - r], S_K + r, S_K + NX - r, at_x(r))
        send(v_ref, vx.at[NX - r], S_V + r, S_V + NX - r, at_x(r))
    for r in (1, 3, 2):
        there = (b + r) % NX
        cols = pl.ds(pl.multiple_of(there * FEATS, FEATS), FEATS)
        send(n_ref.at[:, cols], nx.at[NX - r], S_N + r, S_N + NX - r, at_x(r))
    nx[0] = n_ref[:, pl.ds(pl.multiple_of(b * FEATS, FEATS), FEATS)]

    lane_head = lax.broadcasted_iota(jnp.int32, (BLOCK, WIDTH), 1) // DH
    t_head = lax.broadcasted_iota(jnp.int32, (WIDTH, 2 * BLOCK), 0) // DH
    t_half = lax.broadcasted_iota(jnp.int32, (WIDTH, 2 * BLOCK), 1) // BLOCK

    def lay_out_keys(r, keys, vals):
        for i in range(2):
            j = 2 * r + i
            kb = keys[i * BLOCK : (i + 1) * BLOCK, :]
            vb = vals[i * BLOCK : (i + 1) * BLOCK, :]
            zero = jnp.zeros_like(kb)
            for h in range(HEADS):
                kbd[j, h * DH : (h + 1) * DH, :] = jnp.where(lane_head == h, kb, zero)
                vbd[j, h * DH : (h + 1) * DH, :] = jnp.where(lane_head == h, vb, zero)
            turned = jnp.concatenate([kb, kb], axis=0).T
            for hh in range(HEADS // 2):
                kbt[:, pl.ds(j * WIDTH + hh * ROWS, ROWS)] = jnp.where(
                    t_head == 2 * hh + t_half, turned, jnp.zeros_like(turned)
                )

    lay_out_keys(0, k_ref[...], v_ref[...])

    key_at = lax.broadcasted_iota(jnp.int32, (BLOCK, ROWS), 0)
    row_at = lax.broadcasted_iota(jnp.int32, (BLOCK, ROWS), 1)

    def tile(j, slot, count, own_block=None):
        wide = count * ROWS
        rows = pl.ds(slot * ROWS, wide)
        scores = nt_dot(kbd[j], qa[rows, :])
        gp = nt_dot(vbd[j], ga[rows, :])
        block_id = a * KB + 2 * ((b + j // 2) % NX) + j % 2
        for h in range(HEADS):
            offs = []
            for c in range(count):
                hit = jnp.where(pk[slot + c, h * 8 : (h + 1) * 8, :] == block_id, 1.0, 0.0)
                hit = jnp.max(hit, axis=0, keepdims=True)
                offs.append(jnp.where(hit > 0.5, lm[slot + c, h : h + 1, :], NEVER))
            off = offs[0] if count == 1 else jnp.concatenate(offs, axis=1)
            if own_block is not None:
                ok = key_at <= row_at % BLOCK
                own = jnp.where(ok, jnp.broadcast_to(lm[0, h : h + 1, :], ok.shape), NEVER)
                off = jnp.where(row_at // BLOCK == own_block, own, jnp.broadcast_to(off, ok.shape))
            dots_row = [lm[slot + c, HEADS + h : HEADS + h + 1, :] for c in range(count)]
            dots_row = dots_row[0] if count == 1 else jnp.concatenate(dots_row, axis=1)
            part = slice(h * DH, (h + 1) * DH)
            p = jnp.exp2(scores[part] * (scale * log2e) - off)
            ps[j, part, pl.ds(slot * ROWS, wide)] = p.astype(BF16)
            ds[pl.ds(j * WIDTH + h * DH, DH), pl.ds(slot * ROWS, wide)] = (p * (gp[part] - dots_row)).astype(BF16)

    def tiles(slot, count, first=0):
        def body(j, carry):
            tile(j, slot, count)
            return carry

        lax.fori_loop(first, KB, body, 0)

    def query_grads(slot, count):
        part = nn_dot(kbt[...], ds[:, pl.ds(slot * ROWS, count * ROWS)])
        for c in range(count):
            k = slot + c
            piece = part[:, c * ROWS : (c + 1) * ROWS]
            if k == 0:
                dq0[...] = piece
            else:
                dqs[k] = piece.astype(BF16)
        for c in range(count):
            k = slot + c
            if k:
                send(dqs.at[k], dqr.at[PAIR[k]], S_DQ + k, S_DQ + PAIR[k], at_z(OFFSETS[k]))

    ring_step(1)
    for r in (1, 3, 2):
        arrived(kx.at[r], S_K + r, at_x(r))
        arrived(vx.at[r], S_V + r, at_x(r))
        lay_out_keys(r, kx[r], vx[r])
    for r in (1, 3, 2):
        arrived(nx.at[r], S_N + r, at_x(r))
    ring_step(2)
    for r in range(1, NT):
        send(nx, nt.at[t], S_T + r, S_T + NT - r, at_t(r))
    nt[t] = nx[...]
    for i in range(2):
        tile(i, 0, 1, own_block=i)
    tiles(0, 1, 2)
    query_grads(0, 1)
    tiles(1, 2)
    query_grads(1, 2)
    ring_step(3)
    tiles(3, 2)
    query_grads(3, 2)
    tiles(5, 2)
    query_grads(5, 2)
    ring_step(4)
    tiles(7, 1)
    query_grads(7, 1)

    def key_grads(r):
        for i in range(2):
            j = 2 * r + i
            gv = diagonal_heads(nn_dot(ps[j], ga[...]))
            gk = diagonal_heads(nn_dot(ds[pl.ds(j * WIDTH, WIDTH), :], qa[...])) * scale
            part = slice(i * BLOCK, (i + 1) * BLOCK)
            if r == 0:
                dv0[part, :] = gv
                dk0[part, :] = gk
            else:
                dvs[r, part, :] = gv.astype(BF16)
                dks[r, part, :] = gk.astype(BF16)

    key_grads(1)
    key_grads(2)
    for r in range(1, NT):
        arrived(nt.at[(t + r) % NT], S_T + r, at_t(r))
    for z in range(NZ):
        for r in range(NX):
            ntt[z, :, r * ROWS : (r + 1) * ROWS] = nt[z, r].T

    total = dq0[...]
    for k in range(1, NZ):
        arrived(dqr.at[k], S_DQ + k, at_z(OFFSETS[k]))
    for k in range(1, NZ):
        total = total + dqr[k].astype(F32)
    grad_q = (total * scale).T.astype(BF16)
    dqx[0] = grad_q
    for r in (2, 1, 3):
        send(dqx.at[0], dqx.at[NX - r], S_X + r, S_X + NX - r, at_x(r))
    gq_ref[...] = grad_q
    for r in (1, 2):
        send(dks.at[r], dkr.at[NX - r], S_DK + r, S_DK + NX - r, at_x(r))
        send(dvs.at[r], dvr.at[NX - r], S_DV + r, S_DV + NX - r, at_x(r))
    key_grads(3)
    for r in (3,):
        send(dks.at[r], dkr.at[NX - r], S_DK + r, S_DK + NX - r, at_x(r))
        send(dvs.at[r], dvr.at[NX - r], S_DV + r, S_DV + NX - r, at_x(r))
    key_grads(0)

    for r in (1, 3, 2):
        arrived(dqx.at[r], S_X + r, at_x(r))
    dq_row = dqx[...].reshape(NX * ROWS, WIDTH)
    for k in (7, 5, 6, 3, 4, 1, 2, 0):
        piece = nn_dot(ntt[(a + NZ + OFFSETS[k]) % NZ], dq_row)
        if k == 0:
            gw0[...] = piece
        else:
            gws[k] = piece.astype(BF16)
            send(gws.at[k], gwr.at[PAIR[k]], S_W + k, S_W + PAIR[k], at_z(OFFSETS[k]))

    for r in (1, 3, 2):
        arrived(dkr.at[r], S_DK + r, at_x(r))
        arrived(dvr.at[r], S_DV + r, at_x(r))
    sum_k, sum_v = dk0[...], dv0[...]
    for r in range(1, NX):
        sum_k = sum_k + dkr[r].astype(F32)
        sum_v = sum_v + dvr[r].astype(F32)
    gk_ref[...] = sum_k.astype(BF16)
    gv_ref[...] = sum_v.astype(BF16)

    total_w = gw0[...]
    for k in range(1, NZ):
        arrived(gwr.at[k], S_W + k, at_z(OFFSETS[k]))
    for k in range(1, NZ):
        total_w = total_w + gwr[k].astype(F32)
    gw_ref[...] = total_w
    for copy in started:
        copy.wait_send()


def local(queries, keys, values, attended, cotangent, log_totals, block_picks, normed):
    vmem = pl.BlockSpec(memory_space=pltpu.VMEM)
    sem_count = 4 * NZ + 3 * NX + NT + NZ + 3 * NX + NZ
    b16 = lambda *shape: pltpu.VMEM(shape, BF16)
    f32 = lambda *shape: pltpu.VMEM(shape, F32)
    return pl.pallas_call(
        kernel,
        out_shape=(
            jax.ShapeDtypeStruct((ROWS, WIDTH), BF16),
            jax.ShapeDtypeStruct((ROWS, WIDTH), BF16),
            jax.ShapeDtypeStruct((ROWS, WIDTH), BF16),
            jax.ShapeDtypeStruct((FEATS, WIDTH), F32),
        ),
        in_specs=[vmem] * 6 + [pl.BlockSpec(memory_space=pltpu.SMEM), vmem],
        out_specs=(vmem,) * 4,
        scratch_shapes=[
            b16(NZ * ROWS, WIDTH), b16(NZ * ROWS, WIDTH), f32(NZ, 2 * HEADS, ROWS),
            pltpu.VMEM((NZ, HEADS * SEL, ROWS), jnp.int32),
            b16(NX, ROWS, WIDTH), b16(NX, ROWS, WIDTH),
            b16(KB, WIDTH, WIDTH), b16(KB, WIDTH, WIDTH), b16(WIDTH, KB * WIDTH),
            b16(KB, WIDTH, NZ * ROWS), b16(KB * WIDTH, NZ * ROWS),
            b16(NZ, WIDTH, ROWS), b16(NZ, WIDTH, ROWS), f32(WIDTH, ROWS),
            b16(NX, ROWS, FEATS), b16(NT, NX, ROWS, FEATS), b16(NZ, FEATS, NX * ROWS),
            b16(NX, ROWS, WIDTH),
            b16(NX, ROWS, WIDTH), b16(NX, ROWS, WIDTH), b16(NX, ROWS, WIDTH), b16(NX, ROWS, WIDTH),
            f32(ROWS, WIDTH), f32(ROWS, WIDTH),
            b16(NZ, FEATS, WIDTH), b16(NZ, FEATS, WIDTH), f32(FEATS, WIDTH),
            pltpu.SemaphoreType.DMA((sem_count,)),
            pltpu.SemaphoreType.DMA((sem_count,)),
        ],
        compiler_params=pltpu.CompilerParams(
            collective_id=0, has_side_effects=True, vmem_limit_bytes=48 * 1024 * 1024
        ),
        name="attention_grads",
    )(queries, keys, values, attended, cotangent, log_totals, block_picks, normed)


def solution(mesh):
    in_specs = (
        P("kv", "tp"),
        P("kv", "tp"),
        P("kv", "tp"),
        P("kv", "tp"),
        P("kv", "tp"),
        P("tp", "kv"),
        P("tp", "kv", None),
        P("kv", "tp"),
    )
    out_specs = (P("kv", "tp"), P("kv", "tp"), P("kv", "tp"), P("kv", "tp"))
    return jax.shard_map(local, mesh=mesh, in_specs=in_specs, out_specs=out_specs, check_vma=False)
```

time: 285 us -> 68.8 us (0.24)
  waiting for transfers between devices: 104 us -> 0 us
  Pallas kernels: 0 us -> 58.8 us
  local copies, waits for them, and re-layouts: 66.9 us -> 9 us
  blocking collectives: 42.8 us -> 0 us
  starting transfers between devices: 25.2 us -> 0 us
  matrix products: 22.1 us -> 0 us
  between operations: 15.8 us -> 0.66 us
  other arithmetic: 7.1 us -> 0 us
    all_to_all x3 -> x0, waiting for transfers between devices: 82.6 us -> none  [the longest x2 82.6 us: summed_on_arrival(): lax.all_to_all(parts, axis, split_axis=0, concat_axis=0, tiled=True)]
    pallas_call x0 -> x1, Pallas kernels: none -> 58.8 us  [local(): pl.pallas_call(kernel, out_shape=(jax.ShapeDtypeStruct((ROWS, WIDTH), BF1...]
    all_gather x1 -> x0, blocking collectives: 42.8 us -> none  [in_one_piece(): filled = lax.all_gather(both, axis, axis=dim, tiled=True)]
    reshape x17 -> x0, local copies, waits for them, and re-layouts: 27.5 us -> none  [the longest x11 24.9 us: by_head(): matrix.reshape(blocks, BLOCK, head_count, head_size).transpose(2, 0, 1, 3)]
    all_to_all x3 -> x0, starting transfers between devices: 24.9 us -> none  [the longest x2 13.3 us: summed_on_arrival(): lax.all_to_all(parts, axis, split_axis=0, concat_axis=0, tiled=True)]
    dot_general x12 -> x0, matrix products: 22.1 us -> none  [the longest x1 6.99 us: add_by_block(): jnp.einsum('hnb,hnkd->hbkd', onehot, tiles, precision=lax.Precision.HIGHEST)]
    all_gather x2 -> x0, waiting for transfers between devices: 21 us -> none  [the longest x1 21 us: in_one_piece(): filled = lax.all_gather(both, axis, axis=dim, tiled=True)]
    convert_element_type x8 -> x0, local copies, waits for them, and re-layouts: 19.3 us -> none  [the longest x3 17.4 us: local(): remote_q = summed_on_arrival(dq_full.astype(jnp.bfloat16), 'kv', 0)]
  transfers between devices with their start and end apart: 5 -> 0, of which waited for: 3 -> 0; matrix products, arithmetic and copies ran while one was open for 8% -> 0% of each run, Pallas kernels for 0% -> 0%
where the time goes in v1:
time: 68.8 us; the launch traced here: 68.4 us
  Pallas kernels  58.8 us (85%)
  local copies, waits for them, and re-layouts  9 us (13%)
    pallas_call x1, Pallas kernels, local(): pl.pallas_call(kernel, out_shape=(jax.ShapeDtypeStruct((ROWS, WIDTH), BF1...  58.8 us
    unnamed x20, local copies, waits for them, and re-layouts  9 us

profile of v1, /device:TPU:2, one launch (start us, length us, event | category | flops | bytes accessed | tf_op | source)
XLA Modules:
  0.0 68.4 jit_solution(1678154685314323919)
XLA Ops:
  0.6 0.0 copy-start
  0.6 0.9 %copy-done = bf16[128,512]{1,0:T(8,128)(2,1)S(1)} copy-done((bf16[128,512]{1,0:T(8,128)(2,1)S(1)}, bf16[128,512]{1,0:T(8,128)(2,1)}, u32[]{:S(2)}) %copy-start) | copy-done | bytes 131096
  1.5 0.0 copy-start.1
  1.5 0.8 %copy-done.1 = bf16[128,256]{1,0:T(8,128)(2,1)S(1)} copy-done((bf16[128,256]{1,0:T(8,128)(2,1)S(1)}, bf16[128,256]{1,0:T(8,128)(2,1)}, u32[]{:S(2)}) %copy-start.1) | copy-done | bytes 65560
  2.4 0.0 copy-start.2
  2.4 0.8 %copy-done.2 = bf16[128,256]{1,0:T(8,128)(2,1)S(1)} copy-done((bf16[128,256]{1,0:T(8,128)(2,1)S(1)}, bf16[128,256]{1,0:T(8,128)(2,1)}, u32[]{:S(2)}) %copy-start.2) | copy-done | bytes 65560
  3.2 0.0 copy-start.3
  3.2 0.8 %copy-done.3 = bf16[128,256]{1,0:T(8,128)(2,1)S(1)} copy-done((bf16[128,256]{1,0:T(8,128)(2,1)S(1)}, bf16[128,256]{1,0:T(8,128)(2,1)}, u32[]{:S(2)}) %copy-start.3) | copy-done | bytes 65560
  4.1 0.0 copy-start.4
  4.1 0.8 %copy-done.4 = bf16[128,256]{1,0:T(8,128)(2,1)S(1)} copy-done((bf16[128,256]{1,0:T(8,128)(2,1)S(1)}, bf16[128,256]{1,0:T(8,128)(2,1)}, u32[]{:S(2)}) %copy-start.4) | copy-done | bytes 65560
  4.9 0.0 copy-start.5
  4.9 0.8 %copy-done.5 = bf16[128,256]{1,0:T(8,128)(2,1)S(1)} copy-done((bf16[128,256]{1,0:T(8,128)(2,1)S(1)}, bf16[128,256]{1,0:T(8,128)(2,1)}, u32[]{:S(2)}) %copy-start.5) | copy-done | bytes 65560
  5.7 0.0 copy-start.6
  5.7 0.7 %copy-done.6 = s32[4,2,8]{2,1,0:T(2,128)S(1)} copy-done((s32[4,2,8]{2,1,0:T(2,128)S(1)}, s32[4,2,8]{2,1,0:T(2,128)}, u32[]{:S(2)}) %copy-start.6) | copy-done | bytes 280
  6.4 0.0 copy-start.7
  6.4 0.7 copy-done.7
  7.1 58.8 %attention_grads.1 = (bf16[128,256]{1,0:T(8,128)(2,1)S(1)}, bf16[128,256]{1,0:T(8,128)(2,1)S(1)}, bf16[128,256]{1,0:T(8,128)(2,1)S(1)}, f32[128,256]{1,0:T(8,128)S(1)}) custom-call(bf16[128,256]{1,0:T(8,128)(2,1)S(1)} %copy-done.1, bf16[128,256]{1,0:T(8,128)(2,1)S(1)} %copy-done.2, bf16[128,256]{1,0:T(8,128)(2,1)S(1)} %copy-done.3, ...), custom_call_target="tpu_custom_call" | custom-call | tf_op jit(solution)/shard_map/attention_grads/pallas_call | solution.py:351
  65.9 0.6 copy.16
  66.5 0.6 copy.17
  67.2 0.6 copy.18
  67.8 0.7 copy.19
Async XLA Ops:
  0.6 0.9 %copy-start = (bf16[128,512]{1,0:T(8,128)(2,1)S(1)}, bf16[128,512]{1,0:T(8,128)(2,1)}, u32[]{:S(2)}) copy-start(bf16[128,512]{1,0:T(8,128)(2,1)} %n_ref.1) | copy-start | bytes 393220
  1.5 0.8 %copy-start.1 = (bf16[128,256]{1,0:T(8,128)(2,1)S(1)}, bf16[128,256]{1,0:T(8,128)(2,1)}, u32[]{:S(2)}) copy-start(bf16[128,256]{1,0:T(8,128)(2,1)} %q_ref.1) | copy-start | bytes 196612
  2.4 0.8 %copy-start.2 = (bf16[128,256]{1,0:T(8,128)(2,1)S(1)}, bf16[128,256]{1,0:T(8,128)(2,1)}, u32[]{:S(2)}) copy-start(bf16[128,256]{1,0:T(8,128)(2,1)} %k_ref.1) | copy-start | bytes 196612
  3.2 0.8 %copy-start.3 = (bf16[128,256]{1,0:T(8,128)(2,1)S(1)}, bf16[128,256]{1,0:T(8,128)(2,1)}, u32[]{:S(2)}) copy-start(bf16[128,256]{1,0:T(8,128)(2,1)} %v_ref.1) | copy-start | bytes 196612
  4.1 0.8 %copy-start.4 = (bf16[128,256]{1,0:T(8,128)(2,1)S(1)}, bf16[128,256]{1,0:T(8,128)(2,1)}, u32[]{:S(2)}) copy-start(bf16[128,256]{1,0:T(8,128)(2,1)} %o_ref.1) | copy-start | bytes 196612
  4.9 0.8 %copy-start.5 = (bf16[128,256]{1,0:T(8,128)(2,1)S(1)}, bf16[128,256]{1,0:T(8,128)(2,1)}, u32[]{:S(2)}) copy-start(bf16[128,256]{1,0:T(8,128)(2,1)} %g_ref.1) | copy-start | bytes 196612
  5.7 0.7 %copy-start.6 = (s32[4,2,8]{2,1,0:T(2,128)S(1)}, s32[4,2,8]{2,1,0:T(2,128)}, u32[]{:S(2)}) copy-start(s32[4,2,8]{2,1,0:T(2,128)} %pick_ref.1) | copy-start | bytes 772
  6.4 0.7 copy-start.7

commit v2 on v1

v2 whole, which is shorter than its diff:
```python
import functools
import math

import jax
import jax.numpy as jnp
from jax import lax
from jax.experimental import pallas as pl
from jax.experimental.pallas import tpu as pltpu
from jax.sharding import PartitionSpec as P

MESH = pl.DeviceIdType.MESH
BLOCK = 64
NZ, NX, NT = 8, 4, 8
ROWS = 128
WIDTH = 256
HEADS, DH = 4, 64
SEL = 8
FEATS = 128
KB = 2 * NX
NEVER = 1e30
SEMS = 5 * NZ + 4 * NX + NX + NT + NZ + 3 * NX + NZ
F32, BF16 = jnp.float32, jnp.bfloat16

UP, DOWN = NZ // 2, NZ // 2 - 1


def up_slot(s):
    return 2 * s - 1


def down_slot(s):
    return 2 * s if s < NZ // 2 else NZ - 1


OFFSETS = [0] + [None] * (NZ - 1)
for _s in range(1, NZ // 2 + 1):
    OFFSETS[up_slot(_s)] = -_s
for _s in range(1, NZ // 2):
    OFFSETS[down_slot(_s)] = _s
PAIR = [0] + [OFFSETS.index(-o) if -o in OFFSETS else NZ - 1 for o in OFFSETS[1:]]
FAR_FIRST = sorted(range(NZ), key=lambda k: -abs(OFFSETS[k]))


def nt_dot(a, b):
    return lax.dot_general(a, b, (((1,), (1,)), ((), ())), preferred_element_type=F32)


def nn_dot(a, b):
    return lax.dot_general(a, b, (((1,), (0,)), ((), ())), preferred_element_type=F32)


def diagonal_heads(m):
    lane_head = lax.broadcasted_iota(jnp.int32, (DH, WIDTH), 1) // DH
    out = m[(HEADS - 1) * DH :]
    for h in range(HEADS - 1):
        out = jnp.where(lane_head == h, m[h * DH : (h + 1) * DH], out)
    return out


def kernel(
    q_hbm, k_hbm, v_hbm, o_hbm, g_hbm, l_hbm, pick_hbm, n_hbm,
    gq_hbm, gk_hbm, gv_hbm, gw_hbm,
    gk_ref, gv_ref, gw_ref, o_ref, l_ref, pick_ref, n_ref,
    qa, ga, meta, kx, vx, kbd, vbd, kbt, ps, ds, dqs, dqr, dq0,
    nx, nt, ntt, dqx, dks, dvs, dkr, dvr, dk0, dv0, gws, gwr, gw0,
    load_sem, store_sem, send_sem, recv_sem,
):
    kv = lax.axis_index("kv")
    t = lax.axis_index("tp")
    a = kv // NX
    b = kv % NX
    scale = DH**-0.5
    log2e = 1.0 / math.log(2.0)
    scope = jax.named_scope

    def z_of(off):
        return (a + NZ + off) % NZ

    def at_z(off):
        return {"kv": z_of(off) * NX + b, "tp": t}

    def at_x(r):
        return {"kv": a * NX + (b + r) % NX, "tp": t}

    def at_t(r):
        return {"kv": kv, "tp": (t + r) % NT}

    started = []
    counts = [0]

    def sems(n):
        first = counts[0]
        counts[0] += n
        return first

    S_RING = [sems(NZ) for _ in range(5)]
    S_K, S_V = [sems(NX), sems(NX)], [sems(NX), sems(NX)]
    S_N, S_T = sems(NX), sems(NT)
    S_DQ, S_DK, S_DV, S_X, S_W = sems(NZ), sems(NX), sems(NX), sems(NX), sems(NZ)
    assert counts[0] == SEMS

    def send(src, dst, at_mine, at_theirs, dev, keep=True):
        copy = pltpu.make_async_remote_copy(
            src_ref=src, dst_ref=dst, send_sem=send_sem.at[at_mine], recv_sem=recv_sem.at[at_theirs],
            device_id=dev, device_id_type=MESH,
        )
        copy.start()
        if keep:
            started.append(copy)
        return copy

    def arrived(dst, at_mine, dev):
        pltpu.make_async_remote_copy(
            src_ref=dst, dst_ref=dst, send_sem=send_sem.at[at_mine], recv_sem=recv_sem.at[at_mine],
            device_id=dev, device_id_type=MESH,
        ).wait_recv()

    def slot_rows(slot):
        return pl.ds(slot * ROWS, ROWS)

    def half(ref, slot, i):
        return ref.at[pl.ds(slot * ROWS + i * BLOCK, BLOCK), :]

    own_cols = pl.ds(pl.multiple_of(b * FEATS, FEATS), FEATS)
    loads = [
        pltpu.make_async_copy(src, dst, load_sem.at[i])
        for i, (src, dst) in enumerate((
            (q_hbm, qa.at[slot_rows(0), :]), (g_hbm, ga.at[slot_rows(0), :]), (k_hbm, kx.at[0]), (v_hbm, vx.at[0]),
            (o_hbm, o_ref), (l_hbm, l_ref), (pick_hbm, pick_ref), (n_hbm, n_ref), (n_hbm.at[:, own_cols], nx.at[0]),
        ))
    ]
    for copy in loads:
        copy.start()

    barrier = pltpu.get_barrier_semaphore()
    peers = [at_t(r) for r in range(1, NT)] + [at_x(r) for r in range(1, NX)] + [at_z(1), at_z(-1)]
    for dev in peers:
        pl.semaphore_signal(barrier, inc=1, device_id=dev, device_id_type=MESH)
    with scope("load"):
        for copy in loads:
            copy.wait()

    prod = ga[slot_rows(0), :].astype(F32) * o_ref[...].astype(F32)
    high = prod.astype(BF16)
    low = (prod - high.astype(F32)).astype(BF16)
    ones = (
        lax.broadcasted_iota(jnp.int32, (8, WIDTH), 1) // DH == lax.broadcasted_iota(jnp.int32, (8, WIDTH), 0)
    ).astype(BF16)
    dots = nt_dot(ones, high) + nt_dot(ones, low)
    meta[0, 0:HEADS, :] = l_ref[...] * log2e
    meta[0, HEADS : 2 * HEADS, :] = dots[0:HEADS]
    meta[0, 8:16, :] = jnp.full((8, ROWS), -2.0, F32)
    for h in range(HEADS):
        meta[0, 8 + 2 * h : 10 + 2 * h, 0:SEL] = pick_ref[h].astype(F32)

    with scope("barrier"):
        pl.semaphore_wait(barrier, len(peers))

    up_order = [("m", UP), ("q0", UP), ("q1", UP), ("g0", DOWN), ("g1", DOWN)]
    down_order = [("g0", UP), ("g1", UP), ("m", DOWN), ("q0", DOWN), ("q1", DOWN)]
    names = ["m", "q0", "q1", "g0", "g1"]

    def piece_at(name, slot):
        if name == "m":
            return meta.at[slot]
        return half(qa if name[0] == "q" else ga, slot, int(name[1]))

    def ring_step(s):
        for pieces in zip(up_order, down_order):
            for (name, limit), slot_of, to in zip(pieces, (up_slot, down_slot), (1, -1)):
                sem = S_RING[names.index(name)]
                if 0 < s <= limit:
                    arrived(piece_at(name, slot_of(s)), sem + slot_of(s), at_z(-to))
                if s < limit:
                    there = slot_of(s + 1)
                    src = piece_at(name, slot_of(s) if s else 0)
                    send(src, piece_at(name, there), sem + there, sem + there, at_z(to))

    def key_half(ref, r, i):
        return ref.at[r, pl.ds(i * BLOCK, BLOCK), :]

    def send_keys(ref, first, r, i, source=0):
        there = (source - r) % NX
        send(key_half(ref, source, i), key_half(ref, there, i), first[i] + there, first[i] + there, at_x(r))

    def keys_arrived(ref, first, r, i):
        arrived(key_half(ref, r, i), first[i] + r, at_x(r))

    with scope("start"):
        ring_step(0)
        for i in range(2):
            send_keys(kx, S_K, 1, i)
            send_keys(vx, S_V, 3, i)
        for i in range(2):
            send_keys(vx, S_V, 1, i)
            send_keys(kx, S_K, 3, i)
        for r in (1, 3, 2):
            there = (b + r) % NX
            cols = pl.ds(pl.multiple_of(there * FEATS, FEATS), FEATS)
            send(n_ref.at[:, cols], nx.at[NX - r], S_N + r, S_N + NX - r, at_x(r))

    lane_head = lax.broadcasted_iota(jnp.int32, (BLOCK, WIDTH), 1) // DH
    t_head = lax.broadcasted_iota(jnp.int32, (WIDTH, 2 * BLOCK), 0) // DH
    t_half = lax.broadcasted_iota(jnp.int32, (WIDTH, 2 * BLOCK), 1) // BLOCK

    def lay_out_keys(r):
        for i in range(2):
            j = 2 * r + i
            kb = kx[r, i * BLOCK : (i + 1) * BLOCK, :]
            vb = vx[r, i * BLOCK : (i + 1) * BLOCK, :]
            zero = jnp.zeros_like(kb)
            for h in range(HEADS):
                kbd[j, h * DH : (h + 1) * DH, :] = jnp.where(lane_head == h, kb, zero)
                vbd[j, h * DH : (h + 1) * DH, :] = jnp.where(lane_head == h, vb, zero)
            turned = jnp.concatenate([kb, kb], axis=0).T
            for hh in range(HEADS // 2):
                kbt[:, pl.ds(j * WIDTH + hh * ROWS, ROWS)] = jnp.where(
                    t_head == 2 * hh + t_half, turned, jnp.zeros_like(turned)
                )

    with scope("lay0"):
        lay_out_keys(0)

    key_at = lax.broadcasted_iota(jnp.int32, (BLOCK, ROWS), 0)
    row_at = lax.broadcasted_iota(jnp.int32, (BLOCK, ROWS), 1)
    first_block = lax.broadcasted_iota(jnp.int32, (1, ROWS), 1) < BLOCK

    def side_by_side(parts):
        return parts[0] if len(parts) == 1 else jnp.concatenate(parts, axis=1)

    def tile(j, slot, count, own_block=None):
        wide = count * ROWS
        rows = pl.ds(slot * ROWS, wide)
        scores = nt_dot(kbd[j], qa[rows, :])
        gp = nt_dot(vbd[j], ga[rows, :])
        block_id = (a * KB + 2 * ((b + j // 2) % NX) + j % 2).astype(F32)
        hits = [
            jnp.max(jnp.where(meta[slot + c, 8:16, :] == block_id, 1.0, 0.0), axis=1, keepdims=True)
            for c in range(count)
        ]
        for h in range(HEADS):
            offs = []
            for hit, c in zip(hits, range(count)):
                named = jnp.where(first_block, hit[2 * h : 2 * h + 1, :], hit[2 * h + 1 : 2 * h + 2, :]) > 0.5
                offs.append(jnp.where(named, meta[slot + c, h : h + 1, :], NEVER))
            off = side_by_side(offs)
            if own_block is not None:
                ok = key_at <= row_at % BLOCK
                own = jnp.where(ok, jnp.broadcast_to(meta[0, h : h + 1, :], ok.shape), NEVER)
                off = jnp.where(row_at // BLOCK == own_block, own, jnp.broadcast_to(off, ok.shape))
            dots_row = side_by_side([meta[slot + c, HEADS + h : HEADS + h + 1, :] for c in range(count)])
            part = slice(h * DH, (h + 1) * DH)
            p = jnp.exp2(scores[part] * (scale * log2e) - off)
            ps[j, part, pl.ds(slot * ROWS, wide)] = p.astype(BF16)
            ds[pl.ds(j * WIDTH + h * DH, DH), pl.ds(slot * ROWS, wide)] = (p * (gp[part] - dots_row)).astype(BF16)

    def tiles(slot, count, js):
        for j in js:
            tile(j, slot, count)

    def query_grads(slot, count):
        part = nn_dot(kbt[...], ds[:, pl.ds(slot * ROWS, count * ROWS)])
        for c in range(count):
            k = slot + c
            piece = part[:, c * ROWS : (c + 1) * ROWS]
            if k == 0:
                dq0[...] = piece
            else:
                dqs[k] = piece.astype(BF16)
        for c in range(count):
            k = slot + c
            if k:

                @pl.when(z_of(OFFSETS[k]) > a)
                def _(k=k):
                    send(dqs.at[k], dqr.at[PAIR[k]], S_DQ + k, S_DQ + PAIR[k], at_z(OFFSETS[k]), keep=False)

    with scope("own_tiles"):
        for i in range(2):
            tile(i, 0, 1, own_block=i)
    with scope("keys_pass_on"):
        for i in range(2):
            keys_arrived(kx, S_K, 3, i)
            send_keys(kx, S_K, 1, i, source=3)
            keys_arrived(vx, S_V, 1, i)
            send_keys(vx, S_V, 3, i, source=1)
    with scope("ring1"):
        ring_step(1)
    with scope("keys_near"):
        for i in range(2):
            keys_arrived(vx, S_V, 3, i)
            keys_arrived(kx, S_K, 1, i)
        lay_out_keys(1)
        lay_out_keys(3)
    with scope("tiles_a"):
        tiles(1, 2, (0, 1, 2, 3, 6, 7))
        tiles(0, 1, (2, 3, 6, 7))
    with scope("ring2"):
        ring_step(2)
    with scope("keys_far"):
        for i in range(2):
            keys_arrived(kx, S_K, 2, i)
            keys_arrived(vx, S_V, 2, i)
        lay_out_keys(2)
    with scope("nx"):
        for r in (1, 3, 2):
            arrived(nx.at[r], S_N + r, at_x(r))
        for r in range(1, NT):
            send(nx, nt.at[t], S_T + r, S_T + NT - r, at_t(r))
        nt[t] = nx[...]
    with scope("tiles_b"):
        tiles(1, 2, (4, 5))
        query_grads(1, 2)
        tiles(3, 2, range(KB))
        query_grads(3, 2)
    with scope("ring3"):
        ring_step(3)
    with scope("tiles_c"):
        tiles(0, 1, (4, 5))
        query_grads(0, 1)
        tiles(5, 2, range(KB))
        query_grads(5, 2)
    with scope("ring4"):
        ring_step(4)
    with scope("tiles_d"):
        tiles(7, 1, range(KB))
        query_grads(7, 1)

    def key_grads(r):
        for i in range(2):
            j = 2 * r + i
            gv = diagonal_heads(nn_dot(ps[j], ga[...]))
            gk = diagonal_heads(nn_dot(ds[pl.ds(j * WIDTH, WIDTH), :], qa[...])) * scale
            part = slice(i * BLOCK, (i + 1) * BLOCK)
            if r == 0:
                dv0[part, :] = gv
                dk0[part, :] = gk
            else:
                dvs[r, part, :] = gv.astype(BF16)
                dks[r, part, :] = gk.astype(BF16)

    def send_key_grads(r):
        send(dks.at[r], dkr.at[NX - r], S_DK + r, S_DK + NX - r, at_x(r))
        send(dvs.at[r], dvr.at[NX - r], S_DV + r, S_DV + NX - r, at_x(r))

    with scope("key_grads_a"):
        key_grads(2)
        key_grads(1)
    with scope("nt"):
        for r in range(1, NT):
            arrived(nt.at[(t + r) % NT], S_T + r, at_t(r))
        for i, k in enumerate(FAR_FIRST):
            z = z_of(OFFSETS[k])
            for r in range(NX):
                ntt[i * FEATS : (i + 1) * FEATS, r * ROWS : (r + 1) * ROWS] = nt[z, r].T

    with scope("dq_wait"):
        for k in range(1, NZ):

            @pl.when(z_of(OFFSETS[k]) < a)
            def _(k=k):
                arrived(dqr.at[k], S_DQ + k, at_z(OFFSETS[k]))
                dq0[...] += dqr[k].astype(F32)

    with scope("dq_out"):
        dqx[0] = (dq0[...] * scale).T.astype(BF16)
        for r in (2, 1, 3):
            send(dqx.at[0], dqx.at[NX - r], S_X + r, S_X + NX - r, at_x(r))
    stores = [
        pltpu.make_async_copy(src, dst, store_sem.at[i])
        for i, (src, dst) in enumerate(((dqx.at[0], gq_hbm), (gk_ref, gk_hbm), (gv_ref, gv_hbm), (gw_ref, gw_hbm)))
    ]
    stores[0].start()
    send_key_grads(2)
    send_key_grads(1)
    with scope("key_grads_b"):
        key_grads(3)
        send_key_grads(3)
        key_grads(0)

    with scope("dqx"):
        for r in (1, 3, 2):
            arrived(dqx.at[r], S_X + r, at_x(r))
    with scope("gw"):
        dq_row = dqx[...].reshape(NX * ROWS, WIDTH)
        for first in (0, NZ // 2):
            terms = nn_dot(ntt[first * FEATS : (first + NZ // 2) * FEATS, :], dq_row)
            for i, k in enumerate(FAR_FIRST[first : first + NZ // 2]):
                term = terms[i * FEATS : (i + 1) * FEATS]
                if k == 0:
                    gw0[...] = term
                else:
                    gws[k] = term.astype(BF16)
                    send(gws.at[k], gwr.at[PAIR[k]], S_W + k, S_W + PAIR[k], at_z(OFFSETS[k]))

    with scope("dkv_wait"):
        for r in (1, 3, 2):
            arrived(dkr.at[r], S_DK + r, at_x(r))
            arrived(dvr.at[r], S_DV + r, at_x(r))
        sum_k, sum_v = dk0[...], dv0[...]
        for r in range(1, NX):
            sum_k = sum_k + dkr[r].astype(F32)
            sum_v = sum_v + dvr[r].astype(F32)
        gk_ref[...] = sum_k.astype(BF16)
        gv_ref[...] = sum_v.astype(BF16)
        stores[1].start()
        stores[2].start()

    with scope("gw_wait"):
        total_w = gw0[...]
        for k in range(1, NZ):
            arrived(gwr.at[k], S_W + k, at_z(OFFSETS[k]))
        for k in range(1, NZ):
            total_w = total_w + gwr[k].astype(F32)
        gw_ref[...] = total_w
        stores[3].start()
    with scope("end"):
        for k in range(1, NZ):

            @pl.when(z_of(OFFSETS[k]) > a)
            def _(k=k):
                pltpu.make_async_remote_copy(
                    src_ref=dqs.at[k], dst_ref=dqr.at[PAIR[k]], send_sem=send_sem.at[S_DQ + k],
                    recv_sem=recv_sem.at[S_DQ + PAIR[k]], device_id=at_z(OFFSETS[k]), device_id_type=MESH,
                ).wait_send()

        for copy in started:
            copy.wait_send()
        for copy in stores:
            copy.wait()


def put_out(*refs):
    ins, outs, held, sem = refs[:4], refs[4:8], refs[8:12], refs[12]
    loads = [pltpu.make_async_copy(ins[i], held[i], sem.at[i]) for i in range(4)]
    stores = [pltpu.make_async_copy(held[i], outs[i], sem.at[4 + i]) for i in range(4)]
    for copy in loads:
        copy.start()
    for load, store in zip(loads, stores):
        load.wait()
        store.start()
    for copy in stores:
        copy.wait()


def local(queries, keys, values, attended, cotangent, log_totals, block_picks, normed):
    hbm = pl.BlockSpec(memory_space=pltpu.HBM)
    b16 = lambda *shape: pltpu.VMEM(shape, BF16)
    f32 = lambda *shape: pltpu.VMEM(shape, F32)
    shapes = (
        jax.ShapeDtypeStruct((ROWS, WIDTH), BF16),
        jax.ShapeDtypeStruct((ROWS, WIDTH), BF16),
        jax.ShapeDtypeStruct((ROWS, WIDTH), BF16),
        jax.ShapeDtypeStruct((FEATS, WIDTH), F32),
    )
    grads = pl.pallas_call(
        kernel,
        out_shape=shapes,
        in_specs=[hbm] * 8,
        out_specs=(hbm,) * 4,
        scratch_shapes=[
            b16(ROWS, WIDTH), b16(ROWS, WIDTH), f32(FEATS, WIDTH),
            b16(ROWS, WIDTH), f32(HEADS, ROWS), pltpu.VMEM((HEADS, 2, SEL), jnp.int32), b16(ROWS, NX * FEATS),
            b16(NZ * ROWS, WIDTH), b16(NZ * ROWS, WIDTH), f32(NZ, 16, ROWS),
            b16(NX, ROWS, WIDTH), b16(NX, ROWS, WIDTH),
            b16(KB, WIDTH, WIDTH), b16(KB, WIDTH, WIDTH), b16(WIDTH, KB * WIDTH),
            b16(KB, WIDTH, NZ * ROWS), b16(KB * WIDTH, NZ * ROWS),
            b16(NZ, WIDTH, ROWS), b16(NZ, WIDTH, ROWS), f32(WIDTH, ROWS),
            b16(NX, ROWS, FEATS), b16(NT, NX, ROWS, FEATS), b16(NZ * FEATS, NX * ROWS),
            b16(NX, ROWS, WIDTH),
            b16(NX, ROWS, WIDTH), b16(NX, ROWS, WIDTH), b16(NX, ROWS, WIDTH), b16(NX, ROWS, WIDTH),
            f32(ROWS, WIDTH), f32(ROWS, WIDTH),
            b16(NZ, FEATS, WIDTH), b16(NZ, FEATS, WIDTH), f32(FEATS, WIDTH),
            pltpu.SemaphoreType.DMA((9,)),
            pltpu.SemaphoreType.DMA((4,)),
            pltpu.SemaphoreType.DMA((SEMS,)),
            pltpu.SemaphoreType.DMA((SEMS,)),
        ],
        compiler_params=pltpu.CompilerParams(
            collective_id=0, has_side_effects=True, vmem_limit_bytes=67043328
        ),
        name="attention_grads",
    )(queries, keys, values, attended, cotangent, log_totals, block_picks, normed)
    return pl.pallas_call(
        put_out,
        out_shape=shapes,
        in_specs=[hbm] * 4,
        out_specs=(hbm,) * 4,
        scratch_shapes=[*[b16(ROWS, WIDTH)] * 3, f32(FEATS, WIDTH), pltpu.SemaphoreType.DMA((8,))],
        compiler_params=pltpu.CompilerParams(vmem_limit_bytes=67043328),
        name="put_out",
    )(*grads)


def solution(mesh):
    in_specs = (
        P("kv", "tp"),
        P("kv", "tp"),
        P("kv", "tp"),
        P("kv", "tp"),
        P("kv", "tp"),
        P("tp", "kv"),
        P("tp", "kv", None),
        P("kv", "tp"),
    )
    out_specs = (P("kv", "tp"), P("kv", "tp"), P("kv", "tp"), P("kv", "tp"))
    return jax.shard_map(local, mesh=mesh, in_specs=in_specs, out_specs=out_specs, check_vma=False)
```

time: 68.8 us -> 55.5 us (0.81)
  local copies, waits for them, and re-layouts: 9 us -> 0 us
  Pallas kernels: 58.8 us -> 53.9 us
    unnamed x20 -> x0, local copies, waits for them, and re-layouts: 9 us -> none
    pallas_call x1 -> x2, Pallas kernels: 58.8 us -> 53.9 us  [the longest x1 52.1 us: local(): pl.pallas_call(kernel, out_shape=shapes, in_specs=[hbm] * 8, out_specs=(h...]
where the time goes in v2:
time: 55.5 us; the launch traced here: 54.5 us
  Pallas kernels  53.9 us (97%)
  between operations  0.64 us (1%)
    pallas_call x1, Pallas kernels, local(): pl.pallas_call(kernel, out_shape=shapes, in_specs=[hbm] * 8, out_specs=(h...  52.1 us
    pallas_call x1, Pallas kernels, local(): pl.pallas_call(put_out, out_shape=shapes, in_specs=[hbm] * 4, out_specs=(...  1.73 us

profile of v2, /device:TPU:2, one launch (start us, length us, event | category | flops | bytes accessed | tf_op | source)
XLA Modules:
  0.0 54.5 jit_solution(15412054757736648534)
XLA Ops:
  0.6 52.1 %attention_grads.1 = (bf16[128,256]{1,0:T(8,128)(2,1)}, bf16[128,256]{1,0:T(8,128)(2,1)}, bf16[128,256]{1,0:T(8,128)(2,1)}, f32[128,256]{1,0:T(8,128)}) custom-call(bf16[128,256]{1,0:T(8,128)(2,1)} %q_hbm.1, bf16[128,256]{1,0:T(8,128)(2,1)} %k_hbm.1, bf16[128,256]{1,0:T(8,128)(2,1)} %v_hbm.1, bf16[128,256]{1,0:T(8,128)(2,1)} %o_hbm.1, ...), custom_call_target="tpu_custom_call" | custom-call | tf_op jit(solution)/shard_map/attention_grads/pallas_call | solution.py:456
  52.8 1.7 %put_out.1 = (bf16[128,256]{1,0:T(8,128)(2,1)}, bf16[128,256]{1,0:T(8,128)(2,1)}, bf16[128,256]{1,0:T(8,128)(2,1)}, f32[128,256]{1,0:T(8,128)}) custom-call(bf16[128,256]{1,0:T(8,128)(2,1)} %get-tuple-element.8.refs_0_, bf16[128,256]{1,0:T(8,128)(2,1)} %get-tuple-element.9.refs_1_, bf16[128,256]{1,0:T(8,128)(2,1)} %get-tuple-element.10.refs_2_, ...), custom_call_target="tpu_custom_call" | custom-call | tf_op jit(solution)/shard_map/put_out/pallas_call | solution.py:484

commit v3 on v2

v3 whole, which is shorter than its diff:
```python
import functools
import math

import jax
import jax.numpy as jnp
from jax import lax
from jax.experimental import pallas as pl
from jax.experimental.pallas import tpu as pltpu
from jax.sharding import PartitionSpec as P

MESH = pl.DeviceIdType.MESH
BLOCK = 64
NZ, NX, NT = 8, 4, 8
ROWS = 128
WIDTH = 256
HEADS, DH = 4, 64
SEL = 8
FEATS = 128
KB = 2 * NX
NEVER = 1e30
MAIN_VMEM = 67043328 - (3 * 64 + 128) * 1024
SENDS, ARRIVALS = 28, 63
HALF = WIDTH // 2
F32, BF16 = jnp.float32, jnp.bfloat16

UP, DOWN = NZ // 2, NZ // 2 - 1


def up_slot(s):
    return 2 * s - 1


def down_slot(s):
    return 2 * s if s < NZ // 2 else NZ - 1


OFFSETS = [0] + [None] * (NZ - 1)
for _s in range(1, NZ // 2 + 1):
    OFFSETS[up_slot(_s)] = -_s
for _s in range(1, NZ // 2):
    OFFSETS[down_slot(_s)] = _s
PAIR = [0] + [OFFSETS.index(-o) if -o in OFFSETS else NZ - 1 for o in OFFSETS[1:]]
TERMS = (7, 5, 6, 1, 2, 3, 4, 0)


def nt_dot(a, b):
    return lax.dot_general(a, b, (((1,), (1,)), ((), ())), preferred_element_type=F32)


def nn_dot(a, b):
    return lax.dot_general(a, b, (((1,), (0,)), ((), ())), preferred_element_type=F32)


def diagonal_heads(m):
    lane_head = lax.broadcasted_iota(jnp.int32, (DH, WIDTH), 1) // DH
    out = m[(HEADS - 1) * DH :]
    for h in range(HEADS - 1):
        out = jnp.where(lane_head == h, m[h * DH : (h + 1) * DH], out)
    return out


def kernel(
    q_hbm, k_hbm, v_hbm, o_hbm, g_hbm, l_hbm, pick_hbm, n_hbm,
    gq_ref, gk_ref, gv_ref, gw_ref,
    o_ref, l_ref, pick_ref, n_ref,
    qa, ga, meta, offs, kx, vx, kbd, vbd, kbt, ps, ds, dqs, dqr, dq0,
    nx, nt, ntt, dqx, dks, dvs, dkr, dvr, dk0, dv0, gws, gwr, gw3, gw4, gw_own,
    load_sem, send_sem, recv_sem, go_sem,
):
    kv = lax.axis_index("kv")
    t = lax.axis_index("tp")
    a = kv // NX
    b = kv % NX
    scale = DH**-0.5
    log2e = 1.0 / math.log(2.0)
    scope = jax.named_scope

    def z_of(off):
        return (a + NZ + off) % NZ

    def at_z(off):
        return {"kv": z_of(off) * NX + b, "tp": t}

    def at_x(r):
        return {"kv": a * NX + (b + r) % NX, "tp": t}

    def at_t(r):
        return {"kv": kv, "tp": (t + r) % NT}

    counts = [0, 0]

    def take(which, n):
        first = counts[which]
        counts[which] += n
        return first

    def arrivals(n=1):
        return take(1, n)

    class Sends:
        def __init__(self, cond=None):
            self.at, self.cond, self.size = take(0, 1), cond, 0
            groups.append(self)

        def finish(self):
            like = qa if self.size <= 2 * NZ * ROWS * WIDTH else ds
            ref = like.at[pl.ds(0, self.size // (2 * like.shape[1])), :]
            copy = pltpu.make_async_remote_copy(
                src_ref=ref, dst_ref=ref, send_sem=send_sem.at[self.at], recv_sem=recv_sem.at[0],
                device_id=at_x(1), device_id_type=MESH,
            )
            when(self.cond, copy.wait_send)

    groups = []

    S_RING = [arrivals(NZ - 1) - 1 for _ in range(5)]
    S_K = [(arrivals(), arrivals()) if r == 3 else (arrivals(),) * 2 for r in range(1, NX)]
    S_V = [(arrivals(), arrivals()) if r == 1 else (arrivals(),) * 2 for r in range(1, NX)]
    S_N, S_T, S_DQ, S_DK, S_DV, S_X = arrivals(), arrivals(), arrivals(NZ - 1) - 1, arrivals(), arrivals(), arrivals(2)
    S_W3, S_W4, S_W = (arrivals(2), arrivals(2)), arrivals(2), arrivals()

    def when(cond, do):
        if cond is None:
            do()
        else:
            pl.when(cond)(do)

    def send(src, dst, group, at_theirs, dev, counted=False):
        copy = pltpu.make_async_remote_copy(
            src_ref=src, dst_ref=dst, send_sem=send_sem.at[group.at], recv_sem=recv_sem.at[at_theirs],
            device_id=dev, device_id_type=MESH,
        )
        when(group.cond, copy.start)
        group.size += 0 if counted else math.prod(src.shape) * jnp.dtype(src.dtype).itemsize

    def arrived(dst, at_mine, dev):
        pltpu.make_async_remote_copy(
            src_ref=dst, dst_ref=dst, send_sem=send_sem.at[0], recv_sem=recv_sem.at[at_mine],
            device_id=dev, device_id_type=MESH,
        ).wait_recv()

    def slot_rows(slot):
        return pl.ds(slot * ROWS, ROWS)

    def half(ref, slot, i):
        return ref.at[pl.ds(slot * ROWS + i * BLOCK, BLOCK), :]

    own_cols = pl.ds(pl.multiple_of(b * FEATS, FEATS), FEATS)
    loads = [
        pltpu.make_async_copy(src, dst, load_sem.at[i])
        for i, (src, dst) in enumerate((
            (q_hbm, qa.at[slot_rows(0), :]), (g_hbm, ga.at[slot_rows(0), :]), (k_hbm, kx.at[0]), (v_hbm, vx.at[0]),
            (o_hbm, o_ref), (l_hbm, l_ref), (pick_hbm, pick_ref), (n_hbm, n_ref), (n_hbm.at[:, own_cols], nx.at[0]),
        ))
    ]
    for copy in loads:
        copy.start()

    barrier = pltpu.get_barrier_semaphore()
    peers = [at_t(r) for r in range(1, NT)] + [at_x(r) for r in range(1, NX)] + [at_z(1), at_z(-1)]
    for dev in peers:
        pl.semaphore_signal(barrier, inc=1, device_id=dev, device_id_type=MESH)
    with scope("load"):
        for copy in loads:
            copy.wait()

    prod = ga[slot_rows(0), :].astype(F32) * o_ref[...].astype(F32)
    high = prod.astype(BF16)
    low = (prod - high.astype(F32)).astype(BF16)
    ones = (
        lax.broadcasted_iota(jnp.int32, (8, WIDTH), 1) // DH == lax.broadcasted_iota(jnp.int32, (8, WIDTH), 0)
    ).astype(BF16)
    dots = nt_dot(ones, high) + nt_dot(ones, low)
    meta[0, 0:HEADS, :] = l_ref[...] * log2e
    meta[0, HEADS : 2 * HEADS, :] = dots[0:HEADS]
    meta[0, 8:16, :] = jnp.full((8, ROWS), -2.0, F32)
    for h in range(HEADS):
        for c in range(2):
            meta[0, 8 + c * HEADS + h : 9 + c * HEADS + h, 0:SEL] = pick_ref[h, c : c + 1, :].astype(F32)

    first_block = lax.broadcasted_iota(jnp.int32, (HEADS, ROWS), 1) < BLOCK

    def offsets(slot):
        for j in range(KB):
            block_id = (a * KB + 2 * ((b + j // 2) % NX) + j % 2).astype(F32)
            hit = jnp.where(meta[slot, 8:16, :] == block_id, 1.0, 0.0)
            hit = jnp.max(hit, axis=1, keepdims=True)
            named = jnp.where(first_block, hit[0:HEADS], hit[HEADS : 2 * HEADS]) > 0.5
            offs[slot, j, 0:HEADS, :] = jnp.where(named, meta[slot, 0:HEADS, :], NEVER)

    with scope("barrier"):
        pl.semaphore_wait(barrier, len(peers))

    up_order = [("m", UP), ("q0", UP), ("q1", UP), ("g0", DOWN), ("g1", DOWN)]
    down_order = [("g0", UP), ("g1", UP), ("m", DOWN), ("q0", DOWN), ("q1", DOWN)]
    names = ["m", "q0", "q1", "g0", "g1"]

    def piece_at(name, slot):
        if name == "m":
            return meta.at[slot]
        return half(qa if name[0] == "q" else ga, slot, int(name[1]))

    def flows(down, limit, s):
        return a + s < NZ if down else z_of(-s) >= NZ - limit

    def flows_on(down, limit, s):
        return jnp.logical_and(a + s < NZ, a >= 1) if down else z_of(-s) >= NZ - limit

    def clear(ref):
        ref[...] = jnp.zeros(ref.shape, ref.dtype)

    def ring_step(s, between=(), each=2):
        between = list(between)
        sends = {
            (down, limit): Sends(flows_on(down, limit, s)) for down in (False, True) for limit in (UP, DOWN) if s < limit
        }
        for pieces in zip(up_order, down_order):
            for (name, limit), down in zip(pieces, (False, True)):
                sem = S_RING[names.index(name)]
                slot_of, to = (down_slot, -1) if down else (up_slot, 1)
                if 0 < s <= limit:
                    piece, at, comes = piece_at(name, slot_of(s)), sem + slot_of(s), flows(down, limit, s)
                    pl.when(comes)(functools.partial(arrived, piece, at, at_z(-to)))
                    pl.when(jnp.logical_not(comes))(functools.partial(clear, piece))
                    if name == "m":
                        offsets(slot_of(s))
                if s < limit:
                    there = slot_of(s + 1)
                    src = piece_at(name, slot_of(s) if s else 0)
                    send(src, piece_at(name, there), sends[down, limit], sem + there, at_z(to))
            for do in between[:each]:
                do()
            between = between[each:]
        for do in between:
            do()

    def key_half(ref, r, i):
        return ref.at[r, pl.ds(i * BLOCK, BLOCK), :]

    def send_keys(ref, first, r, i, source=0):
        there = (source - r) % NX
        send(key_half(ref, source, i), key_half(ref, there, i), key_sends, first[there - 1][i], at_x(r))

    def key_half_arrived(ref, first, r, i):
        arrived(key_half(ref, r, i), first[r - 1][i], at_x(r))

    def keys_arrived(ref, first, r):
        arrived(ref.at[r], first[r - 1][0], at_x(r))

    key_sends, n_sends, t_sends, x_sends = Sends(), Sends(), Sends(), Sends()
    with scope("start"):
        ring_step(0)
        for i in range(2):
            send_keys(kx, S_K, 1, i)
            send_keys(vx, S_V, 3, i)
        for i in range(2):
            send_keys(vx, S_V, 1, i)
            send_keys(kx, S_K, 3, i)
        for r in (1, 3, 2):
            there = (b + r) % NX
            cols = pl.ds(pl.multiple_of(there * FEATS, FEATS), FEATS)
            send(n_ref.at[:, cols], nx.at[NX - r], n_sends, S_N, at_x(r))

    lane_head = lax.broadcasted_iota(jnp.int32, (BLOCK, WIDTH), 1) // DH
    t_head = lax.broadcasted_iota(jnp.int32, (WIDTH, 2 * BLOCK), 0) // DH
    t_half = lax.broadcasted_iota(jnp.int32, (WIDTH, 2 * BLOCK), 1) // BLOCK

    def lay_out_keys(r):
        for i in range(2):
            j = 2 * r + i
            kb = kx[r, i * BLOCK : (i + 1) * BLOCK, :]
            vb = vx[r, i * BLOCK : (i + 1) * BLOCK, :]
            zero = jnp.zeros_like(kb)
            for h in range(HEADS):
                kbd[j, h * DH : (h + 1) * DH, :] = jnp.where(lane_head == h, kb, zero)
                vbd[j, h * DH : (h + 1) * DH, :] = jnp.where(lane_head == h, vb, zero)
            turned = jnp.concatenate([kb, kb], axis=0).T
            for hh in range(HEADS // 2):
                kbt[:, pl.ds(j * WIDTH + hh * ROWS, ROWS)] = jnp.where(
                    t_head == 2 * hh + t_half, turned, jnp.zeros_like(turned)
                )

    with scope("lay0"):
        lay_out_keys(0)
        offsets(0)

    key_at = lax.broadcasted_iota(jnp.int32, (BLOCK, ROWS), 0)
    row_at = lax.broadcasted_iota(jnp.int32, (BLOCK, ROWS), 1)

    def side_by_side(parts):
        return parts[0] if len(parts) == 1 else jnp.concatenate(parts, axis=1)

    def tile(j, slot, count, own_block=None):
        wide = count * ROWS
        rows = pl.ds(slot * ROWS, wide)
        scores = nt_dot(kbd[j], qa[rows, :])
        gp = nt_dot(vbd[j], ga[rows, :])
        for h in range(HEADS):
            off = side_by_side([offs[slot + c, j, h : h + 1, :] for c in range(count)])
            if own_block is not None:
                ok = key_at <= row_at % BLOCK
                own = jnp.where(ok, jnp.broadcast_to(meta[0, h : h + 1, :], ok.shape), NEVER)
                off = jnp.where(row_at // BLOCK == own_block, own, jnp.broadcast_to(off, ok.shape))
            dots_row = side_by_side([meta[slot + c, HEADS + h : HEADS + h + 1, :] for c in range(count)])
            part = slice(h * DH, (h + 1) * DH)
            p = jnp.exp2(scores[part] * (scale * log2e) - off)
            ps[j, part, pl.ds(slot * ROWS, wide)] = p.astype(BF16)
            ds[pl.ds(j * WIDTH + h * DH, DH), pl.ds(slot * ROWS, wide)] = (p * (gp[part] - dots_row)).astype(BF16)

    def tiles(slot, count, js):
        for j in js:
            tile(j, slot, count)

    def query_grads(slot, count):
        part = nn_dot(kbt[...], ds[:, pl.ds(slot * ROWS, count * ROWS)])
        for c in range(count):
            k = slot + c
            piece = part[:, c * ROWS : (c + 1) * ROWS]
            if k == 0:
                dq0[...] = piece
            else:
                dqs[k] = piece.astype(BF16)

    dq_sends = {k: Sends(z_of(OFFSETS[k]) > a) for k in range(1, NZ)}

    def send_query_grads(*slots, rows=None):
        def start():
            for k in slots:
                send(dqs.at[k], dqr.at[PAIR[k]], dq_sends[k], S_DQ + PAIR[k], at_z(OFFSETS[k]), counted=dq_sends[k].size > 0)

        when(rows, start)

    def key_pass_on(i):
        key_half_arrived(kx, S_K, 3, i)
        send_keys(kx, S_K, 1, i, source=3)
        key_half_arrived(vx, S_V, 1, i)
        send_keys(vx, S_V, 3, i, source=1)

    def spread_normed():
        arrived(nx.at[pl.ds(1, NX - 1)], S_N, at_x(1))
        for r in range(1, NT):
            send(nx, nt.at[t], t_sends, S_T, at_t(r))
        nt[t] = nx[...]

    def lazily(do, *args, **kwargs):
        return functools.partial(do, *args, **kwargs)

    with scope("own_tiles"):
        for i in range(2):
            tile(i, 0, 1, own_block=i)
    with scope("ring1"):
        ring_step(1, [lambda: None, lazily(key_pass_on, 0), lazily(key_pass_on, 1)], 1)
    with scope("keys_near"):
        keys_arrived(vx, S_V, 3)
        keys_arrived(kx, S_K, 1)
        lay_out_keys(1)
        lay_out_keys(3)
    with scope("ring2"):
        def last_keys():
            keys_arrived(kx, S_K, 2)
            keys_arrived(vx, S_V, 2)
            lay_out_keys(2)

        def first_grads():
            tiles(1, 2, (4, 5))
            query_grads(1, 2)
            send_query_grads(1, 2, rows=a >= 3)

        work = [
            lazily(tiles, 0, 1, (2, 3)),
            lambda: (spread_normed(), tiles(0, 1, (6, 7))),
            lazily(tiles, 1, 2, (0, 1, 2)),
            lambda: (tiles(1, 2, (3, 6, 7)), last_keys()),
            first_grads,
        ]
        ring_step(2, work, 1)
    with scope("ring3"):
        def second_grads():
            tiles(3, 2, range(4, KB))
            query_grads(3, 2)
            send_query_grads(3, 4)

        work = [
            lambda: None,
            lazily(tiles, 3, 2, (0, 1, 2, 3)),
            lazily(send_query_grads, 2, 1, rows=a < 3),
            second_grads,
        ]
        ring_step(3, work, 1)
    with scope("tiles_c"):
        tiles(5, 2, range(KB))
        query_grads(5, 2)
        send_query_grads(5, 6)

    def farthest():
        ring_step(4)
        tiles(7, 1, range(KB))

    @pl.when(a < NZ // 2)
    def _():
        with scope("farthest"):
            farthest()

    @pl.when(a >= NZ // 2)
    def _():
        cols = pl.ds(7 * ROWS, ROWS)
        ps[:, :, cols] = jnp.zeros((KB, WIDTH, ROWS), BF16)
        ds[:, cols] = jnp.zeros((KB * WIDTH, ROWS), BF16)

    with scope("farthest_dq"):
        query_grads(7, 1)
        send_query_grads(7)
    with scope("own_rest"):
        tiles(0, 1, (4, 5))
        query_grads(0, 1)

    def key_grads(r):
        for i in range(2):
            j = 2 * r + i
            gv = diagonal_heads(nn_dot(ps[j], ga[...]))
            gk = diagonal_heads(nn_dot(ds[pl.ds(j * WIDTH, WIDTH), :], qa[...])) * scale
            part = slice(i * BLOCK, (i + 1) * BLOCK)
            if r == 0:
                dv0[part, :] = gv
                dk0[part, :] = gk
            else:
                dvs[r, part, :] = gv.astype(BF16)
                dks[r, part, :] = gk.astype(BF16)

    def send_key_grads(r):
        send(dks.at[r], dkr.at[NX - r], dkv_sends, S_DK, at_x(r))
        send(dvs.at[r], dvr.at[NX - r], dkv_sends, S_DV, at_x(r))

    dkv_sends, w_sends, w2_sends = Sends(), Sends(), Sends()

    def key_grads_a():
        key_grads(2)
        key_grads(1)

    def turn_normed():
        arrived(nt.at[pl.ds(0, NT - 1)], S_T, at_t(1))
        for i, k in enumerate(TERMS):
            z = z_of(OFFSETS[k])
            for r in range(NX):
                ntt[i * FEATS : (i + 1) * FEATS, r * ROWS : (r + 1) * ROWS] = nt[z, r].T

    def side_work():
        key_grads_a()
        turn_normed()

    with scope("side_a"):
        pl.when(a >= NZ // 2)(side_work)
    with scope("dq_wait"):
        for k in range(1, NZ):

            @pl.when(z_of(OFFSETS[k]) < a)
            def _(k=k):
                arrived(dqr.at[k], S_DQ + k, at_z(OFFSETS[k]))
                dq0[...] += dqr[k].astype(F32)

    @pl.when(a >= NZ // 2)
    def _():
        for z in range(NZ // 2):
            pl.semaphore_signal(go_sem, inc=1, device_id={"kv": z * NX + b, "tp": t}, device_id_type=MESH)

    with scope("dq_out"):
        grad_q = (dq0[...] * scale).T.astype(BF16)
        for c in range(2):
            dqx[c, 0] = grad_q[:, c * HALF : (c + 1) * HALF]
        for c in range(2):
            for r in (2, 1, 3):
                send(dqx.at[c, 0], dqx.at[c, NX - r], x_sends, S_X + c, at_x(r))
        gq_ref[...] = grad_q
    with scope("side_b"):
        pl.when(a < NZ // 2)(side_work)
        key_grads(3)
        key_grads(0)
    def gw_terms(c):
        dq_row = dqx[c].reshape(NX * ROWS, HALF)
        for first in (0, NZ // 2):
            terms = nn_dot(ntt[first * FEATS : (first + NZ // 2) * FEATS, :], dq_row)
            for i, k in enumerate(TERMS[first : first + NZ // 2]):
                term = terms[i * FEATS : (i + 1) * FEATS]
                if k in (0, 3, 4):
                    gw_own[c, (0, 3, 4).index(k)] = term
                    continue
                gws[c, k] = term.astype(BF16)
                if k == 7:
                    send(gws.at[c, k], gw4.at[c], w_sends, S_W4 + c, at_z(4 * c - 2))
                elif k in (5, 6):
                    send(gws.at[c, k], gw3.at[c, k - 5], w_sends, S_W3[c] + k - 5, at_z(-1 if k == 5 else 1))
                else:
                    send(gws.at[c, k], gwr.at[c, PAIR[k]], w_sends, S_W, at_z(OFFSETS[k]))

    def gw_pass_on(c):
        for side in (1 - c, c):
            k = 3 + side
            arrived(gw3.at[c, side], S_W3[c] + side, at_z(1 - 2 * side))
            term = gw_own[c, 1 + side] + gw3[c, side].astype(F32)
            if side == c:
                arrived(gw4.at[c], S_W4 + c, at_z(2 - 4 * c))
                term = term + gw4[c].astype(F32)
            gws[c, k] = term.astype(BF16)
            send(gws.at[c, k], gwr.at[c, PAIR[k]], w2_sends, S_W, at_z(OFFSETS[k]))

    with scope("go"):

        @pl.when(a < NZ // 2)
        def _():
            pl.semaphore_wait(go_sem, NZ // 2)

    for c in range(2):
        with scope(f"dqx{c}"):
            arrived(dqx.at[c, pl.ds(1, NX - 1)], S_X + c, at_x(1))
        with scope(f"gw{c}"):
            gw_terms(c)
    for r in (2, 1, 3):
        send_key_grads(r)
    for c in range(2):
        with scope(f"gw_pass_on{c}"):
            gw_pass_on(c)

    with scope("dkv_wait"):
        arrived(dkr.at[pl.ds(1, NX - 1)], S_DK, at_x(1))
        arrived(dvr.at[pl.ds(1, NX - 1)], S_DV, at_x(1))
        sum_k, sum_v = dk0[...], dv0[...]
        for r in range(1, NX):
            sum_k = sum_k + dkr[r].astype(F32)
            sum_v = sum_v + dvr[r].astype(F32)
        gk_ref[...] = sum_k.astype(BF16)
        gv_ref[...] = sum_v.astype(BF16)

    with scope("gw_wait"):
        arrived(qa.at[pl.ds(0, 4 * ROWS), :], S_W, at_z(1))
        for c in range(2):
            total_w = gw_own[c, 0]
            for k in range(1, 5):
                total_w = total_w + gwr[c, k].astype(F32)
            gw_ref[:, c * HALF : (c + 1) * HALF] = total_w
    with scope("end"):
        for group in groups:
            group.finish()
        assert counts == [SENDS, ARRIVALS], counts


def put_out(*refs):
    stores = [pltpu.make_async_copy(refs[i], refs[4 + i], refs[8].at[i]) for i in range(4)]
    for copy in stores:
        copy.start()
    for copy in stores:
        copy.wait()


def local(queries, keys, values, attended, cotangent, log_totals, block_picks, normed):
    vmem = pl.BlockSpec(memory_space=pltpu.VMEM)
    hbm = pl.BlockSpec(memory_space=pltpu.HBM)
    b16 = lambda *shape: pltpu.VMEM(shape, BF16)
    f32 = lambda *shape: pltpu.VMEM(shape, F32)
    shapes = (
        jax.ShapeDtypeStruct((ROWS, WIDTH), BF16),
        jax.ShapeDtypeStruct((ROWS, WIDTH), BF16),
        jax.ShapeDtypeStruct((ROWS, WIDTH), BF16),
        jax.ShapeDtypeStruct((FEATS, WIDTH), F32),
    )
    grads = pl.pallas_call(
        kernel,
        out_shape=tuple(pltpu.VMEM(x.shape, x.dtype) for x in shapes),
        in_specs=[hbm] * 8,
        out_specs=(vmem,) * 4,
        scratch_shapes=[
            b16(ROWS, WIDTH), f32(HEADS, ROWS), pltpu.VMEM((HEADS, 2, SEL), jnp.int32), b16(ROWS, NX * FEATS),
            b16(NZ * ROWS, WIDTH), b16(NZ * ROWS, WIDTH), f32(NZ, 16, ROWS), f32(NZ, KB, 8, ROWS),
            b16(NX, ROWS, WIDTH), b16(NX, ROWS, WIDTH),
            b16(KB, WIDTH, WIDTH), b16(KB, WIDTH, WIDTH), b16(WIDTH, KB * WIDTH),
            b16(KB, WIDTH, NZ * ROWS), b16(KB * WIDTH, NZ * ROWS),
            b16(NZ, WIDTH, ROWS), b16(NZ, WIDTH, ROWS), f32(WIDTH, ROWS),
            b16(NX, ROWS, FEATS), b16(NT, NX, ROWS, FEATS), b16(NZ * FEATS, NX * ROWS),
            b16(2, NX, ROWS, HALF),
            b16(NX, ROWS, WIDTH), b16(NX, ROWS, WIDTH), b16(NX, ROWS, WIDTH), b16(NX, ROWS, WIDTH),
            f32(ROWS, WIDTH), f32(ROWS, WIDTH),
            b16(2, NZ, FEATS, HALF), b16(2, 5, FEATS, HALF),
            b16(2, 2, FEATS, HALF), b16(2, FEATS, HALF), f32(2, 3, FEATS, HALF),
            pltpu.SemaphoreType.DMA((9,)),
            pltpu.SemaphoreType.DMA((SENDS,)),
            pltpu.SemaphoreType.DMA((ARRIVALS,)),
            pltpu.SemaphoreType.REGULAR,
        ],
        compiler_params=pltpu.CompilerParams(
            collective_id=0, has_side_effects=True, vmem_limit_bytes=MAIN_VMEM
        ),
        name="attention_grads",
    )(queries, keys, values, attended, cotangent, log_totals, block_picks, normed)
    return pl.pallas_call(
        put_out,
        out_shape=shapes,
        in_specs=[vmem] * 4,
        out_specs=(hbm,) * 4,
        scratch_shapes=[pltpu.SemaphoreType.DMA((4,))],
        compiler_params=pltpu.CompilerParams(vmem_limit_bytes=1024 * 1024),
        name="put_out",
    )(*grads)


def solution(mesh):
    in_specs = (
        P("kv", "tp"),
        P("kv", "tp"),
        P("kv", "tp"),
        P("kv", "tp"),
        P("kv", "tp"),
        P("tp", "kv"),
        P("tp", "kv", None),
        P("kv", "tp"),
    )
    out_specs = (P("kv", "tp"), P("kv", "tp"), P("kv", "tp"), P("kv", "tp"))
    return jax.shard_map(local, mesh=mesh, in_specs=in_specs, out_specs=out_specs, check_vma=False)
```

time: 55.5 us -> 49.5 us (0.89)
  Pallas kernels: 53.9 us -> 48.1 us
    pallas_call x2, Pallas kernels: 53.9 us -> 48.1 us  [the longest x1 47.4 us: local(): pl.pallas_call(kernel, out_shape=tuple((pltpu.VMEM(x.shape, x.dtype) for...]
where the time goes in v3:
time: 49.5 us; the launch traced here: 48.8 us
  Pallas kernels  48.1 us (97%)
  between operations  0.64 us (1%)
    pallas_call x1, Pallas kernels, local(): pl.pallas_call(kernel, out_shape=tuple((pltpu.VMEM(x.shape, x.dtype) for...  47.4 us

profile of v3, /device:TPU:2, one launch (start us, length us, event | category | flops | bytes accessed | tf_op | source)
XLA Modules:
  0.0 48.8 jit_solution(426958066270339558)
XLA Ops:
  0.6 47.4 %attention_grads.1 = (bf16[128,256]{1,0:T(8,128)(2,1)S(1)}, bf16[128,256]{1,0:T(8,128)(2,1)S(1)}, bf16[128,256]{1,0:T(8,128)(2,1)S(1)}, f32[128,256]{1,0:T(8,128)S(1)}) custom-call(bf16[128,256]{1,0:T(8,128)(2,1)} %q_hbm.1, bf16[128,256]{1,0:T(8,128)(2,1)} %k_hbm.1, bf16[128,256]{1,0:T(8,128)(2,1)} %v_hbm.1, bf16[128,256]{1,0:T(8,128)(2,1)} %o_hbm.1, ...), custom_call_target="tpu_custom_call" | custom-call | tf_op jit(solution)/shard_map/attention_grads/pallas_call | solution.py:565
  48.0 0.8 %put_out.1 = (bf16[128,256]{1,0:T(8,128)(2,1)}, bf16[128,256]{1,0:T(8,128)(2,1)}, bf16[128,256]{1,0:T(8,128)(2,1)}, f32[128,256]{1,0:T(8,128)}) custom-call(bf16[128,256]{1,0:T(8,128)(2,1)S(1)} %get-tuple-element.8.refs_0_, bf16[128,256]{1,0:T(8,128)(2,1)S(1)} %get-tuple-element.9.refs_1_, bf16[128,256]{1,0:T(8,128)(2,1)S(1)} %get-tuple-element.10.refs_2_, ...), custom_call_target="tpu_custom_call" | custom-call | tf_op jit(solution)/shard_map/put_out/pallas_call | solution.py:593

commit v4 on v3

--- a/solution.py
+++ b/solution.py
@@ -375,16 +375,26 @@
         ]
         ring_step(2, work, 1)
     with scope("ring3"):
-        def second_grads():
-            tiles(3, 2, range(4, KB))
+        def second_tiles(js):
+            tiles(3, 2, js)
+
+        def second_grads(js):
+            tiles(3, 2, js)
             query_grads(3, 2)
-            send_query_grads(3, 4)
+
+        def if_early(do, *args):
+            pl.when(a < 3)(functools.partial(do, *args))
+
+        @pl.when(a >= 3)
+        def _():
+            second_grads(range(KB))
+            send_query_grads(4, 3)
 
         work = [
             lambda: None,
-            lazily(tiles, 3, 2, (0, 1, 2, 3)),
+            lazily(if_early, second_tiles, range(4)),
             lazily(send_query_grads, 2, 1, rows=a < 3),
-            second_grads,
+            lambda: (if_early(second_grads, range(4, KB)), send_query_grads(4, 3, rows=a < 3)),
         ]
         ring_step(3, work, 1)
     with scope("tiles_c"):

time: 49.5 us -> 49.3 us (level)
  no operation moved by 1% of the time
where the time goes in v4:
time: 49.3 us; the launch traced here: 48.4 us
  Pallas kernels  47.8 us (97%)
  between operations  0.64 us (1%)
    pallas_call x1, Pallas kernels, local(): pl.pallas_call(kernel, out_shape=tuple((pltpu.VMEM(x.shape, x.dtype) for...  47 us

profile of v4, /device:TPU:2, one launch (start us, length us, event | category | flops | bytes accessed | tf_op | source)
XLA Modules:
  0.0 48.4 jit_solution(9162793622934934412)
XLA Ops:
  0.6 47.0 %attention_grads.1 = (bf16[128,256]{1,0:T(8,128)(2,1)S(1)}, bf16[128,256]{1,0:T(8,128)(2,1)S(1)}, bf16[128,256]{1,0:T(8,128)(2,1)S(1)}, f32[128,256]{1,0:T(8,128)S(1)}) custom-call(bf16[128,256]{1,0:T(8,128)(2,1)} %q_hbm.1, bf16[128,256]{1,0:T(8,128)(2,1)} %k_hbm.1, bf16[128,256]{1,0:T(8,128)(2,1)} %v_hbm.1, bf16[128,256]{1,0:T(8,128)(2,1)} %o_hbm.1, ...), custom_call_target="tpu_custom_call" | custom-call | tf_op jit(solution)/shard_map/attention_grads/pallas_call | solution.py:575
  47.6 0.8 %put_out.1 = (bf16[128,256]{1,0:T(8,128)(2,1)}, bf16[128,256]{1,0:T(8,128)(2,1)}, bf16[128,256]{1,0:T(8,128)(2,1)}, f32[128,256]{1,0:T(8,128)}) custom-call(bf16[128,256]{1,0:T(8,128)(2,1)S(1)} %get-tuple-element.8.refs_0_, bf16[128,256]{1,0:T(8,128)(2,1)S(1)} %get-tuple-element.9.refs_1_, bf16[128,256]{1,0:T(8,128)(2,1)S(1)} %get-tuple-element.10.refs_2_, ...), custom_call_target="tpu_custom_call" | custom-call | tf_op jit(solution)/shard_map/put_out/pallas_call | solution.py:603

commit v5 on v4

--- a/solution.py
+++ b/solution.py
@@ -19,7 +19,7 @@
 KB = 2 * NX
 NEVER = 1e30
 MAIN_VMEM = 67043328 - (3 * 64 + 128) * 1024
-SENDS, ARRIVALS = 28, 63
+SENDS, ARRIVALS = 28, 64
 HALF = WIDTH // 2
 F32, BF16 = jnp.float32, jnp.bfloat16
 
@@ -40,7 +40,7 @@
 for _s in range(1, NZ // 2):
     OFFSETS[down_slot(_s)] = _s
 PAIR = [0] + [OFFSETS.index(-o) if -o in OFFSETS else NZ - 1 for o in OFFSETS[1:]]
-TERMS = (7, 5, 6, 1, 2, 3, 4, 0)
+TERMS = (7, 6, 5, 2, 1, 3, 4, 0)
 
 
 def nt_dot(a, b):
@@ -63,7 +63,7 @@
     q_hbm, k_hbm, v_hbm, o_hbm, g_hbm, l_hbm, pick_hbm, n_hbm,
     gq_ref, gk_ref, gv_ref, gw_ref,
     o_ref, l_ref, pick_ref, n_ref,
-    qa, ga, meta, offs, kx, vx, kbd, vbd, kbt, ps, ds, dqs, dqr, dq0,
+    qa, ga, meta, offs, kx, vx, kbd, vbd, kbt, ps, ds, dqs, dqr, dqm, dq0,
     nx, nt, ntt, dqx, dks, dvs, dkr, dvr, dk0, dv0, gws, gwr, gw3, gw4, gw_own,
     load_sem, send_sem, recv_sem, go_sem,
 ):
@@ -117,6 +117,7 @@
     S_K = [(arrivals(), arrivals()) if r == 3 else (arrivals(),) * 2 for r in range(1, NX)]
     S_V = [(arrivals(), arrivals()) if r == 1 else (arrivals(),) * 2 for r in range(1, NX)]
     S_N, S_T, S_DQ, S_DK, S_DV, S_X = arrivals(), arrivals(), arrivals(NZ - 1) - 1, arrivals(), arrivals(), arrivals(2)
+    S_DM = arrivals()
     S_W3, S_W4, S_W = (arrivals(2), arrivals(2)), arrivals(2), arrivals()
 
     def when(cond, do):
@@ -326,7 +327,11 @@
     def send_query_grads(*slots, rows=None):
         def start():
             for k in slots:
-                send(dqs.at[k], dqr.at[PAIR[k]], dq_sends[k], S_DQ + PAIR[k], at_z(OFFSETS[k]), counted=dq_sends[k].size > 0)
+                counted = dq_sends[k].size > 0
+                if k == 4:
+                    send(dqs.at[k], dqm, dq_sends[k], S_DM, at_z(1), counted)
+                else:
+                    send(dqs.at[k], dqr.at[PAIR[k]], dq_sends[k], S_DQ + PAIR[k], at_z(OFFSETS[k]), counted)
 
         when(rows, start)
 
@@ -364,7 +369,7 @@
         def first_grads():
             tiles(1, 2, (4, 5))
             query_grads(1, 2)
-            send_query_grads(1, 2, rows=a >= 3)
+            send_query_grads(1, rows=a >= 3)
 
         work = [
             lazily(tiles, 0, 1, (2, 3)),
@@ -393,7 +398,7 @@
         work = [
             lambda: None,
             lazily(if_early, second_tiles, range(4)),
-            lazily(send_query_grads, 2, 1, rows=a < 3),
+            lazily(send_query_grads, 1, rows=a < 3),
             lambda: (if_early(second_grads, range(4, KB)), send_query_grads(4, 3, rows=a < 3)),
         ]
         ring_step(3, work, 1)
@@ -460,8 +465,16 @@
 
     with scope("side_a"):
         pl.when(a >= NZ // 2)(side_work)
+    with scope("dq_merge"):
+
+        @pl.when(jnp.logical_and(a >= 1, a <= NZ - 2))
+        def _():
+            arrived(dqm, S_DM, at_z(-1))
+            dqs[2] = (dqs[2].astype(F32) + dqm[...].astype(F32)).astype(BF16)
+
+        send_query_grads(2)
     with scope("dq_wait"):
-        for k in range(1, NZ):
+        for k in (1, 2, 4, 5, 6, 7):
 
             @pl.when(z_of(OFFSETS[k]) < a)
             def _(k=k):
@@ -487,9 +500,9 @@
         key_grads(0)
     def gw_terms(c):
         dq_row = dqx[c].reshape(NX * ROWS, HALF)
-        for first in (0, NZ // 2):
-            terms = nn_dot(ntt[first * FEATS : (first + NZ // 2) * FEATS, :], dq_row)
-            for i, k in enumerate(TERMS[first : first + NZ // 2]):
+        for first in range(0, NZ, 2):
+            terms = nn_dot(ntt[first * FEATS : (first + 2) * FEATS, :], dq_row)
+            for i, k in enumerate(TERMS[first : first + 2]):
                 term = terms[i * FEATS : (i + 1) * FEATS]
                 if k in (0, 3, 4):
                     gw_own[c, (0, 3, 4).index(k)] = term
@@ -583,7 +596,7 @@
             b16(NX, ROWS, WIDTH), b16(NX, ROWS, WIDTH),
             b16(KB, WIDTH, WIDTH), b16(KB, WIDTH, WIDTH), b16(WIDTH, KB * WIDTH),
             b16(KB, WIDTH, NZ * ROWS), b16(KB * WIDTH, NZ * ROWS),
-            b16(NZ, WIDTH, ROWS), b16(NZ, WIDTH, ROWS), f32(WIDTH, ROWS),
+            b16(NZ, WIDTH, ROWS), b16(NZ, WIDTH, ROWS), b16(WIDTH, ROWS), f32(WIDTH, ROWS),
             b16(NX, ROWS, FEATS), b16(NT, NX, ROWS, FEATS), b16(NZ * FEATS, NX * ROWS),
             b16(2, NX, ROWS, HALF),
             b16(NX, ROWS, WIDTH), b16(NX, ROWS, WIDTH), b16(NX, ROWS, WIDTH), b16(NX, ROWS, WIDTH),

time: 49.3 us -> 49.1 us (level)
  no operation moved by 1% of the time
where the time goes in v5:
time: 49.1 us; the launch traced here: 48.2 us
  Pallas kernels  47.6 us (97%)
  between operations  0.64 us (1%)
    pallas_call x1, Pallas kernels, local(): pl.pallas_call(kernel, out_shape=tuple((pltpu.VMEM(x.shape, x.dtype) for...  46.8 us

profile of v5, /device:TPU:2, one launch (start us, length us, event | category | flops | bytes accessed | tf_op | source)
XLA Modules:
  0.0 48.2 jit_solution(18303747856580472155)
XLA Ops:
  0.6 46.8 %attention_grads.1 = (bf16[128,256]{1,0:T(8,128)(2,1)S(1)}, bf16[128,256]{1,0:T(8,128)(2,1)S(1)}, bf16[128,256]{1,0:T(8,128)(2,1)S(1)}, f32[128,256]{1,0:T(8,128)S(1)}) custom-call(bf16[128,256]{1,0:T(8,128)(2,1)} %q_hbm.1, bf16[128,256]{1,0:T(8,128)(2,1)} %k_hbm.1, bf16[128,256]{1,0:T(8,128)(2,1)} %v_hbm.1, bf16[128,256]{1,0:T(8,128)(2,1)} %o_hbm.1, ...), custom_call_target="tpu_custom_call" | custom-call | tf_op jit(solution)/shard_map/attention_grads/pallas_call | solution.py:588
  47.5 0.8 %put_out.1 = (bf16[128,256]{1,0:T(8,128)(2,1)}, bf16[128,256]{1,0:T(8,128)(2,1)}, bf16[128,256]{1,0:T(8,128)(2,1)}, f32[128,256]{1,0:T(8,128)}) custom-call(bf16[128,256]{1,0:T(8,128)(2,1)S(1)} %get-tuple-element.8.refs_0_, bf16[128,256]{1,0:T(8,128)(2,1)S(1)} %get-tuple-element.9.refs_1_, bf16[128,256]{1,0:T(8,128)(2,1)S(1)} %get-tuple-element.10.refs_2_, ...), custom_call_target="tpu_custom_call" | custom-call | tf_op jit(solution)/shard_map/put_out/pallas_call | solution.py:616

commit v6 on v5

--- a/solution.py
+++ b/solution.py
@@ -512,8 +512,10 @@
                     send(gws.at[c, k], gw4.at[c], w_sends, S_W4 + c, at_z(4 * c - 2))
                 elif k in (5, 6):
                     send(gws.at[c, k], gw3.at[c, k - 5], w_sends, S_W3[c] + k - 5, at_z(-1 if k == 5 else 1))
-                else:
-                    send(gws.at[c, k], gwr.at[c, PAIR[k]], w_sends, S_W, at_z(OFFSETS[k]))
+
+    def send_near_terms(c):
+        for k in (1, 2):
+            send(gws.at[c, k], gwr.at[c, PAIR[k]], w_sends, S_W, at_z(OFFSETS[k]))
 
     def gw_pass_on(c):
         for side in (1 - c, c):
@@ -537,6 +539,8 @@
             arrived(dqx.at[c, pl.ds(1, NX - 1)], S_X + c, at_x(1))
         with scope(f"gw{c}"):
             gw_terms(c)
+    for c in range(2):
+        send_near_terms(c)
     for r in (2, 1, 3):
         send_key_grads(r)
     for c in range(2):

time: 49.1 us -> 48.8 us (level)
  no operation moved by 1% of the time
where the time goes in v6:
time: 48.8 us; the launch traced here: 48.1 us
  Pallas kernels  47.5 us (97%)
  between operations  0.64 us (1%)
    pallas_call x1, Pallas kernels, local(): pl.pallas_call(kernel, out_shape=tuple((pltpu.VMEM(x.shape, x.dtype) for...  46.7 us

profile of v6, /device:TPU:2, one launch (start us, length us, event | category | flops | bytes accessed | tf_op | source)
XLA Modules:
  0.0 48.1 jit_solution(12142668556559714074)
XLA Ops:
  0.6 46.7 %attention_grads.1 = (bf16[128,256]{1,0:T(8,128)(2,1)S(1)}, bf16[128,256]{1,0:T(8,128)(2,1)S(1)}, bf16[128,256]{1,0:T(8,128)(2,1)S(1)}, f32[128,256]{1,0:T(8,128)S(1)}) custom-call(bf16[128,256]{1,0:T(8,128)(2,1)} %q_hbm.1, bf16[128,256]{1,0:T(8,128)(2,1)} %k_hbm.1, bf16[128,256]{1,0:T(8,128)(2,1)} %v_hbm.1, bf16[128,256]{1,0:T(8,128)(2,1)} %o_hbm.1, ...), custom_call_target="tpu_custom_call" | custom-call | tf_op jit(solution)/shard_map/attention_grads/pallas_call | solution.py:592
  47.4 0.8 %put_out.1 = (bf16[128,256]{1,0:T(8,128)(2,1)}, bf16[128,256]{1,0:T(8,128)(2,1)}, bf16[128,256]{1,0:T(8,128)(2,1)}, f32[128,256]{1,0:T(8,128)}) custom-call(bf16[128,256]{1,0:T(8,128)(2,1)S(1)} %get-tuple-element.8.refs_0_, bf16[128,256]{1,0:T(8,128)(2,1)S(1)} %get-tuple-element.9.refs_1_, bf16[128,256]{1,0:T(8,128)(2,1)S(1)} %get-tuple-element.10.refs_2_, ...), custom_call_target="tpu_custom_call" | custom-call | tf_op jit(solution)/shard_map/put_out/pallas_call | solution.py:620
